TPU v7x, 32 devices: a whole 2x2x4 slice. The times are simulated.
32 devices in a mesh: ep: 16 (over z, y, x), tp: 2 (over core).
Axes of the slice: x: 2, y: 2, z: 4, core: 2. Of those that a mesh axis runs over, the one named last changes fastest.
Arguments:
- tokens: bfloat16 [4096, 2048], P('ep'), may hold values from -6 to 6
- expert_ids: int32 [4096, 4], P('ep'), may hold values from 0 to 15, all different within a row; in each aligned block of 256 rows (0 to 255, 256 to 511, ...) at most 96 rows name the same one
- gates: float32 [4096, 4], P('ep'), may hold values from 0.05 to 0.6
- cotangent: bfloat16 [4096, 2048], P('ep'), may hold values from -6 to 6
- w_gate: bfloat16 [16, 2048, 512], P('ep', None, 'tp'), may hold values from -0.125 to 0.125
- w_up: bfloat16 [16, 2048, 512], P('ep', None, 'tp'), may hold values from -0.125 to 0.125
- w_down: bfloat16 [16, 512, 2048], P('ep', 'tp'), may hold values from -0.25 to 0.25
- sh_gate: bfloat16 [2048, 512], P(None, 'tp'), may hold values from -0.125 to 0.125
- sh_up: bfloat16 [2048, 512], P(None, 'tp'), may hold values from -0.125 to 0.125
- sh_down: bfloat16 [512, 2048], P('tp'), may hold values from -0.25 to 0.25
Outputs:
- token_grad: bfloat16 [4096, 2048], P('ep', 'tp')
- gate_grad: float32 [4096, 4], P('ep')
- expert_gate_grad: float32 [16, 2048, 512], P('ep', None, 'tp')
- expert_up_grad: float32 [16, 2048, 512], P('ep', None, 'tp')
- expert_down_grad: float32 [16, 512, 2048], P('ep', 'tp')
- shared_gate_grad: float32 [2048, 512], P('ep', 'tp')
- shared_up_grad: float32 [2048, 512], P('ep', 'tp')
- shared_down_grad: float32 [512, 2048], P('tp', 'ep')
- expert_gate_rows: float32 [16, 2048], P('ep')
- expert_up_rows: float32 [16, 2048], P('ep')
- expert_down_rows: float32 [16, 512], P('ep', 'tp')
- shared_gate_rows: float32 [2048], P('ep')
- shared_up_rows: float32 [2048], P('ep')
- shared_down_rows: float32 [512], P('tp')
Inputs may be any that keep to these rules, and one draw needn't show every extreme that they name: `expert_ids`: each row names 4 different experts. Within each aligned block of 256 tokens no expert is named by more than 96 assignments, a bound that is reached in some blocks.
All inputs are finite; a program needn't handle non-finite values.
Results may differ from a plain program's by a relative error of at most 0.0085.
Values may be sent and summed in bfloat16 or wider, within the bound.
A program may use at most 128 MiB of HBM per device.

v0:
```python
import jax
import jax.numpy as jnp
from jax import lax
from jax.sharding import PartitionSpec as P


def silu_parts(pre):
    sigmoid = jax.nn.sigmoid(pre)
    return (pre * sigmoid, sigmoid * (1.0 + pre * (1.0 - sigmoid)))


def expert_backward(inputs, cot_rows, w_g, w_u, w_d):
    gate_pre = jnp.dot(inputs, w_g, preferred_element_type=jnp.float32)
    up_pre = jnp.dot(inputs, w_u, preferred_element_type=jnp.float32)
    active, slope = silu_parts(gate_pre)
    hidden = (active * up_pre).astype(jnp.bfloat16)
    hidden_cot = jnp.dot(cot_rows, w_d.T, preferred_element_type=jnp.float32)
    gate_part = jnp.sum(hidden.astype(jnp.float32) * hidden_cot, axis=1)
    d_gate = (hidden_cot * up_pre * slope).astype(jnp.bfloat16)
    d_up = (hidden_cot * active).astype(jnp.bfloat16)
    contract = (((0,), (0,)), ((), ()))
    grad_g = lax.dot_general(inputs, d_gate, contract, preferred_element_type=jnp.float32)
    grad_u = lax.dot_general(inputs, d_up, contract, preferred_element_type=jnp.float32)
    grad_d = lax.dot_general(hidden, cot_rows, contract, preferred_element_type=jnp.float32)
    partial_value = jnp.dot(d_gate, w_g.T, preferred_element_type=jnp.float32) + jnp.dot(
        d_up, w_u.T, preferred_element_type=jnp.float32
    )
    return (grad_g, grad_u, grad_d, partial_value, gate_part)


def local(tokens, expert_ids, gates, cotangent, w_gate, w_up, w_down, sh_gate, sh_up, sh_down):
    experts_count = lax.axis_size("ep")
    tok_rows, model_width = tokens.shape
    top_count = expert_ids.shape[1]
    capacity = 3 * tok_rows * top_count // (2 * experts_count)
    assign = tok_rows * top_count
    flat_ids = expert_ids.reshape(assign)
    onehot = (flat_ids[:, None] == jnp.arange(experts_count, dtype=jnp.int32)[None, :]).astype(
        jnp.int32
    )
    slot_rank = jnp.sum((jnp.cumsum(onehot, axis=0) - 1) * onehot, axis=1)
    slot_of = flat_ids * capacity + slot_rank
    slot_table = (
        jnp.full((experts_count * capacity,), assign, jnp.int32)
        .at[slot_of]
        .set(jnp.arange(assign, dtype=jnp.int32))
    )
    filled = slot_table < assign
    source = jnp.minimum(slot_table, assign - 1)
    token_row = source // top_count
    slot_gate = jnp.where(filled, gates.reshape(assign)[source], jnp.zeros((), jnp.float32))
    half_cols = model_width // lax.axis_size("tp")
    first_col = lax.axis_index("tp") * half_cols
    inputs = jnp.where(
        filled[:, None],
        lax.dynamic_slice_in_dim(tokens, first_col, half_cols, 1)[token_row],
        jnp.zeros((), jnp.bfloat16),
    )
    scaled = (
        slot_gate[:, None]
        * lax.dynamic_slice_in_dim(cotangent, first_col, half_cols, 1)[token_row].astype(
            jnp.float32
        )
    ).astype(jnp.bfloat16)
    inputs, scaled = (inputs, scaled)
    part_in, part_cot = (
        lax.all_to_all(inputs, "ep", split_axis=0, concat_axis=0, tiled=True),
        lax.all_to_all(scaled, "ep", split_axis=0, concat_axis=0, tiled=True),
    )
    got_in, got_cot = (
        lax.all_gather(part_in, "tp", axis=1, tiled=True),
        lax.all_gather(part_cot, "tp", axis=1, tiled=True),
    )
    grad_g, grad_u, grad_d, partial_value, gate_part = expert_backward(
        got_in, got_cot, w_gate[0], w_up[0], w_down[0]
    )
    slot_rows = lax.psum_scatter(
        partial_value.astype(jnp.bfloat16), "tp", scatter_dimension=1, tiled=True
    )
    back_rows = lax.all_to_all(slot_rows, "ep", split_axis=0, concat_axis=0, tiled=True)
    shared_grad_g, shared_grad_u, shared_grad_d, partial_value, unused = expert_backward(
        tokens, cotangent, sh_gate, sh_up, sh_down
    )
    shared_g = lax.psum_scatter(shared_grad_g, "ep", scatter_dimension=0, tiled=True)
    shared_u = lax.psum_scatter(shared_grad_u, "ep", scatter_dimension=0, tiled=True)
    shared_d = lax.psum_scatter(shared_grad_d, "ep", scatter_dimension=1, tiled=True)
    down_norms = lax.psum(jnp.sum(shared_d * shared_d, axis=1), "ep")
    shared_rows = lax.psum_scatter(
        partial_value.astype(jnp.bfloat16), "tp", scatter_dimension=1, tiled=True
    ).astype(jnp.float32)
    shared_parts = (shared_g, shared_u, shared_d, down_norms, shared_rows)
    shared_g, shared_u, shared_d, down_norms, shared_rows = shared_parts
    gate_total, gate_norms, up_norms, shared_gate_norms, shared_up_norms = lax.psum(
        (
            gate_part,
            jnp.sum(grad_g * grad_g, axis=1),
            jnp.sum(grad_u * grad_u, axis=1),
            jnp.sum(shared_g * shared_g, axis=1),
            jnp.sum(shared_u * shared_u, axis=1),
        ),
        "tp",
    )
    back_gate = lax.all_to_all(gate_total, "ep", split_axis=0, concat_axis=0, tiled=True)
    picks = slot_of.reshape(tok_rows, top_count)
    routed = jnp.sum(back_rows[picks].astype(jnp.float32), axis=1)
    token_grad = (routed + shared_rows).astype(jnp.bfloat16)
    gate_grad = back_gate[picks] / gates
    return (
        token_grad,
        gate_grad,
        grad_g[None],
        grad_u[None],
        grad_d[None],
        shared_g,
        shared_u,
        shared_d,
        gate_norms[None],
        up_norms[None],
        jnp.sum(grad_d * grad_d, axis=1)[None],
        shared_gate_norms,
        shared_up_norms,
        down_norms,
    )


def solution(mesh):
    placed = (
        P("ep", None),
        P("ep", None),
        P("ep", None),
        P("ep", None),
        P("ep", None, "tp"),
        P("ep", None, "tp"),
        P("ep", "tp", None),
        P(None, "tp"),
        P(None, "tp"),
        P("tp", None),
    )
    return jax.shard_map(
        local,
        mesh=mesh,
        in_specs=placed,
        out_specs=(
            P("ep", "tp"),
            P("ep", None),
            P("ep", None, "tp"),
            P("ep", None, "tp"),
            P("ep", "tp", None),
            P("ep", "tp"),
            P("ep", "tp"),
            P("tp", "ep"),
            P("ep", None),
            P("ep", None),
            P("ep", "tp"),
            P("ep"),
            P("ep"),
            P("tp"),
        ),
        check_vma=False,
    )
```

profile of v0, /device:TPU:0, one launch (start us, length us, event | category | flops | bytes accessed | tf_op | source)
XLA Modules:
  0.0 590.0 jit_solution(12502688182972828595)
XLA Ops:
  9.2 4.5 reduce-window.6
  16.1 4.3 scatter_custom_fusion
  20.5 5.9 gather_fusion
  26.5 5.8 gather_fusion.2
  32.3 2.1 broadcast_select_fusion
  34.4 79.5 %all_to_all.42 = bf16[16,96,1024]{2,1,0:T(8,128)(2,1)} all-to-all(bf16[16,96,1024]{2,1,0:T(8,128)(2,1)S(1)} %broadcast_select_fusion), channel_id=1, replica_groups=mesh['ep'=16,'tp'=2] {'ep'}, dimensions={0} | all-to-all | bytes 6291456 | tf_op jit(solution)/shard_map/all_to_all | solution.py:67
  115.2 5.8 gather_fusion.1
  121.0 3.0 fusion
  124.0 74.5 %all_to_all.43 = bf16[16,96,1024]{2,1,0:T(8,128)(2,1)} all-to-all(bf16[16,96,1024]{2,1,0:T(8,128)(2,1)S(1)} %fusion), channel_id=1, replica_groups=mesh['ep'=16,'tp'=2] {'ep'}, dimensions={0} | all-to-all | bytes 6291456 | tf_op jit(solution)/shard_map/all_to_all | solution.py:68
  206.5 7.2 %fusion.5 = f32[1536,256]{0,1:T(8,128)} fusion(bf16[1536,2048]{1,0:T(8,128)(2,1)} %all-gather.5.cloned.1.call-done, bf16[1,2048,256]{2,1,0:T(8,128)(2,1)S(1)} %copy-done), kind=kOutput, calls=%fused_computation.25 | convolution fusion | flops 1610612736 | bytes 8912896 | tf_op jit(solution)/shard_map/dot_general | solution.py:13
  213.7 3.0 fusion.8
  216.8 7.3 %multiply_reduce_fusion.3 = (f32[1536]{0:T(1024)S(1)}, bf16[1536,256]{0,1:T(8,128)(2,1)}, bf16[1536,256]{0,1:T(8,128)(2,1)S(1)}, bf16[1536,256]{0,1:T(8,128)(2,1)S(1)}) fusion(f32[1536,256]{0,1:T(8,128)} %fusion.8, f32[1536,256]{0,1:T(8,128)} %fusion.5, bf16[1536,2048]{1,0:T(8,128)(2,1)} %all-gather.3.cloned.1.call-done, bf16[1,256,2048]{2,1,0:T(8,128)(2,1)} %param.16), kind=kOutput, calls=%fused_computation.17 | convolution fusion | flops 1617689088 | bytes 12851200 | tf_op jit(solution)/shard_map/dot_general | solution.py:17
  224.1 1.9 fusion.3
  225.9 4.5 add_convert_fusion
  231.6 1.9 fusion.13
  233.5 50.8 %reduce-scatter.12.cloned.1.call-done = f32[128,256]{0,1:T(8,128)} async-done(((f32[2048,256]{0,1:T(8,128)}), f32[128,256]{0,1:T(8,128)}) %reduce-scatter.12.cloned.1.call-update) | async-done | bytes 131088 | tf_op jit(solution)/shard_map/reduce_scatter | solution.py:85
  285.2 79.7 %reduce-scatter.10.cloned.1.call-done = f32[128,256]{0,1:T(8,128)} async-done(((f32[2048,256]{0,1:T(8,128)}), f32[128,256]{0,1:T(8,128)}) %reduce-scatter.10.cloned.1.call-update) | async-done | bytes 131088 | tf_op jit(solution)/shard_map/reduce_scatter | solution.py:84
  366.0 5.9 multiply_reduce_fusion.2
  371.9 7.6 %multiply_reduce_fusion.1 = (f32[2048]{0:T(1024)S(1)}, f32[2048,256]{0,1:T(8,128)}) fusion(bf16[1536,256]{0,1:T(8,128)(2,1)S(1)} %get-tuple-element.66, bf16[1536,2048]{1,0:T(8,128)(2,1)} %all-gather.5.cloned.1.call-done), kind=kOutput, calls=%fused_computation.15 | convolution fusion | flops 1611659264 | bytes 9183232 | tf_op jit(solution)/shard_map/dot_general | solution.py:23
  379.5 4.0 all-reduce
  383.4 9.9 %all_to_all.44 = f32[16,96,1]{1,2,0:T(1,128)S(1)} all-to-all(f32[16,96,1]{1,2,0:T(1,128)S(1)} %bitcast.90), channel_id=1, replica_groups=mesh['ep'=16,'tp'=2] {'ep'}, dimensions={0} | all-to-all | bytes 12288 | tf_op jit(solution)/shard_map/all_to_all | solution.py:103
  393.3 3.7 all-to-all-start.2
  403.9 97.8 %reduce-scatter.14.cloned.1.call-done = f32[256,128]{1,0:T(8,128)} async-done(((f32[256,2048]{1,0:T(8,128)}), f32[256,128]{1,0:T(8,128)}) %reduce-scatter.14.cloned.1.call-update) | async-done | bytes 131088 | tf_op jit(solution)/shard_map/reduce_scatter | solution.py:86
  502.7 42.0 %psum.47 = f32[256]{0:T(256)} all-reduce(f32[256]{0:T(256)S(1)} %multiply_reduce_fusion.4), channel_id=1, replica_groups=mesh['ep'=16,'tp'=2] {'ep'}, use_global_device_ids=true, to_apply=%region_22.23 | all-reduce | flops 256 | bytes 2048 | tf_op jit(solution)/shard_map/psum | solution.py:87
  544.7 2.9 copy.52
  547.6 2.9 copy.51
  550.5 6.7 %multiply_reduce_fusion = (f32[256]{0:T(256)}, f32[256,2048]{1,0:T(8,128)}) fusion(bf16[1536,256]{0,1:T(8,128)(2,1)} %get-tuple-element.62, bf16[1536,2048]{1,0:T(8,128)(2,1)} %all-gather.3.cloned.1.call-done), kind=kOutput, calls=%fused_computation.14 | convolution fusion | flops 1611661056 | bytes 9176064 | tf_op jit(solution)/shard_map/dot_general | solution.py:24
  558.5 6.1 %gather_fusion.4 = f32[1024]{0:T(1024)S(1)} fusion(f32[1536]{0:T(1024)S(1)} %all_to_all.37, s32[1024]{0:T(1024)S(1)} %broadcast_clamp_fusion), kind=kCustom, calls=%fused_computation.4 | custom fusion | bytes 12288 | tf_op jit(solution)/shard_map/gather | solution.py:107
  565.5 5.4 gather_fusion.3
  570.8 4.8 reshape.163
  575.7 4.7 reduce_sum.88
  580.5 2.0 add_convert_fusion.1
  (87 shorter events, 25.9 us)
Async XLA Ops:
  8.0 198.5 %copy-start = (bf16[1,2048,256]{2,1,0:T(8,128)(2,1)S(1)}, bf16[1,2048,256]{2,1,0:T(8,128)(2,1)}, u32[]{:S(2)}) copy-start(bf16[1,2048,256]{2,1,0:T(8,128)(2,1)} %param.14) | copy-start | bytes 3145732
  8.0 198.5 %all-gather.5.cloned.1.call-start = ((), (), s32[]{:S(2)}) async-start(), calls=%async_computation.10 | async-start | bytes 9437184 | tf_op jit(solution)/shard_map/all_gather | solution.py:71
  20.5 6.0 %copy-start.2 = (bf16[256,2048]{1,0:T(8,128)(2,1)S(1)}, bf16[256,2048]{1,0:T(8,128)(2,1)}, u32[]{:S(2)}) copy-start(bf16[256,2048]{1,0:T(8,128)(2,1)} %param.10) | copy-start | bytes 3145732
  114.0 102.8 %all-gather.3.cloned.1.call-start = ((), (), s32[]{:S(2)}) async-start(), calls=%async_computation.9 | async-start | bytes 9437184 | tf_op jit(solution)/shard_map/all_gather | solution.py:72
  198.5 85.7 %reduce-scatter.12.cloned.1.call-start = ((), (), s32[]{:S(2)}) async-start(), calls=%async_computation.14 | async-start | bytes 2228224 | tf_op jit(solution)/shard_map/reduce_scatter | solution.py:85
  198.6 3.5 copy-start.4
  198.6 3.5 copy-start.10
  204.4 160.6 %reduce-scatter.10.cloned.1.call-start = ((), (), s32[]{:S(2)}) async-start(), calls=%async_computation.13 | async-start | bytes 2228224 | tf_op jit(solution)/shard_map/reduce_scatter | solution.py:84
  206.2 7.5 %copy-start.6 = (bf16[1,2048,256]{2,1,0:T(8,128)(2,1)S(1)}, bf16[1,2048,256]{2,1,0:T(8,128)(2,1)}, u32[]{:S(2)}) copy-start(bf16[1,2048,256]{2,1,0:T(8,128)(2,1)} %param.15) | copy-start | bytes 3145732
  206.3 187.1 %reduce-scatter.6.cloned.1.call-start = ((), (), s32[]{:S(2)}) async-start(), calls=%async_computation.11 | async-start | bytes 9437184 | tf_op jit(solution)/shard_map/reduce_scatter | solution.py:77
  206.5 7.2 %copy-start.9 = (bf16[1536,2048]{1,0:T(8,128)(2,1)S(1)}, bf16[1536,2048]{1,0:T(8,128)(2,1)}, u32[]{:S(2)}) copy-start(bf16[1536,2048]{1,0:T(8,128)(2,1)} %all-gather.5.cloned.1.call-done) | copy-start | bytes 18874372
  224.1 1.9 copy-start.7
  230.4 1.2 copy-start.5
  230.4 271.3 %reduce-scatter.14.cloned.1.call-start = ((), (), s32[]{:S(2)}) async-start(), calls=%async_computation.15 | async-start | bytes 2228224 | tf_op jit(solution)/shard_map/reduce_scatter | solution.py:86
  393.3 172.2 %all-to-all-start.2 = ((bf16[16,96,1024]{2,1,0:T(8,128)(2,1)}), bf16[16,96,1024]{2,1,0:T(8,128)(2,1)S(1)}, u32[]{:S(2)}, u32[]{:S(2)}) async-start(bf16[16,96,1024]{2,1,0:T(8,128)(2,1)} %bitcast.82), calls=%async_computation.3 | async-start | bytes 6291456 | tf_op jit(solution)/shard_map/all_to_all | solution.py:80
  397.1 183.4 %reduce-scatter.8.cloned.1.call-start = ((), (), s32[]{:S(2)}) async-start(), calls=%async_computation.12 | async-start | bytes 1572864 | tf_op jit(solution)/shard_map/reduce_scatter | solution.py:88
  397.1 1.8 copy-start.3
  398.9 2.6 copy-start.8
  570.8 11.6 %copy-start.1 = (bf16[1,2048,256]{2,1,0:T(8,128)(2,1)S(1)}, bf16[1,2048,256]{2,1,0:T(8,128)(2,1)}, u32[]{:S(2)}) copy-start(bf16[1,2048,256]{2,1,0:T(8,128)(2,1)} %param.14) | copy-start | bytes 3145732
Sparse Core Ops, SparseCore 0:
  114.1 15.0 all-gather.4
  198.6 15.0 all-gather.2
Sparse Core Ops, SparseCore 1:
  204.5 79.7 reduce-scatter.11
  287.0 77.9 reduce-scatter.9
  367.1 10.6 reduce-scatter.5
  380.6 121.0 reduce-scatter.13
  504.0 9.0 reduce-scatter.7
where the time goes:
time: 591 us; the launch traced here: 590 us
  waiting for transfers between devices  228 us (39%)
  blocking collectives  210 us (36%)
  matrix products  56.7 us (10%)
  local copies, waits for them, and re-layouts  53.7 us (9%)
  other arithmetic  20.9 us (4%)
  between operations  16.1 us (3%)
    reduce_scatter x1, waiting for transfers between devices, local(): lax.psum_scatter(shared_grad_d, 'ep', scatter_dimension=1, tiled=True)  97.8 us
    reduce_scatter x1, waiting for transfers between devices, local(): lax.psum_scatter(shared_grad_g, 'ep', scatter_dimension=0, tiled=True)  79.7 us
    all_to_all x1, blocking collectives, local(): lax.all_to_all(inputs, 'ep', split_axis=0, concat_axis=0, tiled=True)  79.5 us
    all_to_all x1, blocking collectives, local(): lax.all_to_all(scaled, 'ep', split_axis=0, concat_axis=0, tiled=True)  74.5 us
    reduce_scatter x1, waiting for transfers between devices, local(): lax.psum_scatter(shared_grad_u, 'ep', scatter_dimension=0, tiled=True)  50.8 us
    psum x1, blocking collectives, local(): down_norms = lax.psum(jnp.sum(shared_d * shared_d, axis=1), 'ep')  42 us
  transfers between devices with their start and end apart: 8, of which 3 were waited for; matrix products, arithmetic and copies ran while one was open for 17% of the time, Pallas kernels for 0%

commit v1 on v0

v1 whole, which is shorter than its diff:
```python
import functools
import math

import jax
import jax.numpy as jnp
from jax import lax
from jax.experimental import pallas as pl
from jax.experimental.pallas import tpu as pltpu
from jax.sharding import PartitionSpec as P

BF16 = jnp.bfloat16
F32 = jnp.float32


def silu_parts(pre):
    sigmoid = jax.nn.sigmoid(pre)
    return (pre * sigmoid, sigmoid * (1.0 + pre * (1.0 - sigmoid)))


def expert_backward(inputs, cot_rows, w_g, w_u, w_d):
    gate_pre = jnp.dot(inputs, w_g, preferred_element_type=F32)
    up_pre = jnp.dot(inputs, w_u, preferred_element_type=F32)
    active, slope = silu_parts(gate_pre)
    hidden = (active * up_pre).astype(BF16)
    hidden_cot = jnp.dot(cot_rows, w_d.T, preferred_element_type=F32)
    gate_part = jnp.sum(hidden.astype(F32) * hidden_cot, axis=1)
    d_gate = (hidden_cot * up_pre * slope).astype(BF16)
    d_up = (hidden_cot * active).astype(BF16)
    contract = (((0,), (0,)), ((), ()))
    grad_g = lax.dot_general(inputs, d_gate, contract, preferred_element_type=F32)
    grad_u = lax.dot_general(inputs, d_up, contract, preferred_element_type=F32)
    grad_d = lax.dot_general(hidden, cot_rows, contract, preferred_element_type=F32)
    partial_value = jnp.dot(d_gate, w_g.T, preferred_element_type=F32) + jnp.dot(
        d_up, w_u.T, preferred_element_type=F32
    )
    return (grad_g, grad_u, grad_d, partial_value.astype(BF16), gate_part)


def plane_count(mesh):
    count = mesh.shape["ep"]
    try:
        planes = len({tuple(d.coords)[2] for d in mesh.devices.flat})
    except (AttributeError, TypeError, IndexError):
        planes = 0
    if planes < 1 or count % planes:
        planes = max(d for d in range(1, math.isqrt(count) + 1) if count % d == 0)
    return planes


def copy_to(src, dst, send, recv, ep, tp):
    return pltpu.make_async_remote_copy(
        src_ref=src,
        dst_ref=dst,
        send_sem=send,
        recv_sem=recv,
        device_id=(ep, tp),
        device_id_type=pl.DeviceIdType.MESH,
    )


def combine_kernel(
    planes, width,
    own, oth, sh_own, sh_oth, scatter, grads,
    tok_out, grad_out,
    tp_in, sh_in, sums, plane_in, gplane_in, z_out, z_in, gz_out, gz_in, routed, gtotal,
    tp_sem, plane_sem, gplane_sem, z_sem, gz_sem,
):
    me, core = lax.axis_index("ep"), lax.axis_index("tp")
    z, q = me // width, me % width
    order = list(range(1, planes)) + [0]
    dest_z = [(z + step) % planes for step in order]
    dest_q = [(q + step) % width for step in range(width)]
    started = []

    def start(copy):
        copy.start()
        started.append(copy)
        return copy

    tp_copies = [
        start(copy_to(oth.at[dest_z[i]], tp_in.at[i], tp_sem.at[0, i], tp_sem.at[1, i], me, 1 - core))
        for i in range(planes)
    ]
    sh_copy = start(
        copy_to(sh_oth, sh_in, tp_sem.at[0, planes], tp_sem.at[1, planes], me, 1 - core)
    )
    plane_copies, gplane_copies = {}, {}
    for i in range(planes):
        for d in range(1, width):
            peer = z * width + dest_q[d]
            gplane_copies[i, d] = start(
                copy_to(
                    grads.at[dest_z[i], dest_q[d]],
                    gplane_in.at[i, d - 1],
                    gplane_sem.at[0, i, d - 1],
                    gplane_sem.at[1, i, d - 1],
                    peer,
                    core,
                )
            )
        tp_copies[i].wait_recv()
        for d in range(width):
            sums[i, d] = (
                own[dest_z[i], dest_q[d]].astype(F32) + tp_in[i, dest_q[d]].astype(F32)
            ).astype(BF16)
            if d:
                peer = z * width + dest_q[d]
                plane_copies[i, d] = start(
                    copy_to(
                        sums.at[i, d],
                        plane_in.at[i, d - 1],
                        plane_sem.at[0, i, d - 1],
                        plane_sem.at[1, i, d - 1],
                        peer,
                        core,
                    )
                )
    z_copies = []
    for i in range(planes):
        peer = dest_z[i] * width + q
        total = grads[dest_z[i], q].astype(F32)
        for d in range(1, width):
            gplane_copies[i, d].wait_recv()
            total = total + gplane_in[i, d - 1].astype(F32)
        if i < planes - 1:
            gz_out[i] = total.astype(BF16)
            z_copies.append(
                start(copy_to(gz_out.at[i], gz_in.at[i], gz_sem.at[0, i], gz_sem.at[1, i], peer, core))
            )
        else:
            gtotal[...] = total
        for d in range(1, width):
            plane_copies[i, d].wait_recv()
        acc = jnp.dot(scatter[dest_z[i], 0], sums[i, 0], preferred_element_type=F32)
        for d in range(1, width):
            acc = acc + jnp.dot(
                scatter[dest_z[i], d], plane_in[i, d - 1], preferred_element_type=F32
            )
        if i < planes - 1:
            z_out[i] = acc.astype(BF16)
            z_copies.append(
                start(copy_to(z_out.at[i], z_in.at[i], z_sem.at[0, i], z_sem.at[1, i], peer, core))
            )
        else:
            routed[...] = acc
    sh_copy.wait_recv()
    for copy in z_copies:
        copy.wait_recv()
    total = gtotal[...]
    acc = routed[...]
    for i in range(planes - 1):
        total = total + gz_in[i].astype(F32)
        acc = acc + z_in[i].astype(F32)
    grad_out[...] = total
    acc = acc + (sh_own[...].astype(F32) + sh_in[...].astype(F32))
    tok_out[...] = acc.astype(BF16)
    for copy in started:
        copy.wait_send()


def combine(planes, own, oth, sh_own, sh_oth, scatter, grads):
    width = own.shape[1]
    cap, cols = own.shape[2:]
    rows = sh_own.shape[0]
    g_shape = grads.shape[2:]
    vmem = pl.BlockSpec(memory_space=pltpu.VMEM)
    far, side = max(planes - 1, 1), max(width - 1, 1)
    return pl.pallas_call(
        functools.partial(combine_kernel, planes, width),
        out_shape=(
            jax.ShapeDtypeStruct((rows, cols), BF16),
            jax.ShapeDtypeStruct(g_shape, F32),
        ),
        in_specs=[vmem] * 6,
        out_specs=(vmem, vmem),
        scratch_shapes=[
            pltpu.VMEM((planes, width, cap, cols), BF16),
            pltpu.VMEM((rows, cols), BF16),
            pltpu.VMEM((planes, width, cap, cols), BF16),
            pltpu.VMEM((planes, side, cap, cols), BF16),
            pltpu.VMEM((planes, side) + g_shape, BF16),
            pltpu.VMEM((far, rows, cols), BF16),
            pltpu.VMEM((far, rows, cols), BF16),
            pltpu.VMEM((far,) + g_shape, BF16),
            pltpu.VMEM((far,) + g_shape, BF16),
            pltpu.VMEM((rows, cols), F32),
            pltpu.VMEM(g_shape, F32),
            pltpu.SemaphoreType.DMA((2, planes + 1)),
            pltpu.SemaphoreType.DMA((2, planes, side)),
            pltpu.SemaphoreType.DMA((2, planes, side)),
            pltpu.SemaphoreType.DMA((2, far)),
            pltpu.SemaphoreType.DMA((2, far)),
        ],
        compiler_params=pltpu.CompilerParams(
            has_side_effects=True, vmem_limit_bytes=60 * 2**20
        ),
        name="combine",
    )(own, oth, sh_own, sh_oth, scatter, grads)


def local(planes, tokens, expert_ids, gates, cotangent, w_gate, w_up, w_down, sh_gate, sh_up, sh_down):
    experts_count = lax.axis_size("ep")
    width = experts_count // planes
    me, core = lax.axis_index("ep"), lax.axis_index("tp")
    z, q = me // width, me % width
    tok_rows, model_width = tokens.shape
    top_count = expert_ids.shape[1]
    capacity = 3 * tok_rows * top_count // (2 * experts_count)
    half_cols = model_width // lax.axis_size("tp")
    first_col = core * half_cols

    all_ids = lax.all_gather(expert_ids, "ep", axis=0)
    line_ids = lax.dynamic_index_in_dim(
        all_ids.reshape(planes, width, tok_rows, top_count), q, 1, keepdims=False
    )
    lanes = jnp.arange(experts_count, dtype=jnp.int32)
    earlier = jnp.tril(jnp.ones((tok_rows, tok_rows), BF16), -1)

    def ranks_of(names):
        rank = jnp.dot(earlier, names.astype(BF16), preferred_element_type=F32)
        return jnp.where(names, rank.astype(jnp.int32), -1)

    mine = expert_ids[:, :, None] == lanes
    rank = ranks_of(jnp.any(mine, axis=1))
    gate_of = jnp.sum(jnp.where(mine, gates[:, :, None], 0.0), axis=1)
    slots = jnp.arange(capacity, dtype=jnp.int32)
    picked = rank.T[:, None, :] == slots[None, :, None]
    slot_gate = jnp.sum(jnp.where(picked, gate_of.T[:, None, :], 0.0), axis=2)
    picked_rows = picked.astype(BF16).reshape(experts_count * capacity, tok_rows)

    tok_half = lax.dynamic_slice_in_dim(tokens, first_col, half_cols, 1)
    cot_half = lax.dynamic_slice_in_dim(cotangent, first_col, half_cols, 1)
    inputs = jnp.dot(picked_rows, tok_half, preferred_element_type=F32).astype(BF16)
    scaled = (
        jnp.dot(picked_rows, cot_half, preferred_element_type=F32) * slot_gate.reshape(-1, 1)
    ).astype(BF16)
    part_in, part_cot = (
        lax.all_to_all(inputs, "ep", split_axis=0, concat_axis=0, tiled=True),
        lax.all_to_all(scaled, "ep", split_axis=0, concat_axis=0, tiled=True),
    )
    got_in, got_cot = (
        lax.all_gather(part_in, "tp", axis=1, tiled=True),
        lax.all_gather(part_cot, "tp", axis=1, tiled=True),
    )
    shared_g, shared_u, shared_d, shared_part, unused = expert_backward(
        tokens, cotangent, sh_gate, sh_up, sh_down
    )
    grad_g, grad_u, grad_d, routed_part, gate_part = expert_backward(
        got_in, got_cot, w_gate[0], w_up[0], w_down[0]
    )

    part_rows = model_width // experts_count
    hidden_cols = sh_gate.shape[1]
    pieces = hidden_cols // part_rows
    deal = (planes, width, part_rows, hidden_cols)
    down = shared_d.astype(BF16).reshape(pieces, part_rows, experts_count, part_rows)
    down = down.transpose(2, 1, 0, 3).reshape(deal)
    grads = jnp.concatenate(
        [shared_g.astype(BF16).reshape(deal), shared_u.astype(BF16).reshape(deal), down], axis=2
    )

    senders = z * width + (q - jnp.arange(width, dtype=jnp.int32)) % width
    named = line_ids[:, :, :, None] == senders
    named = jnp.any(named, axis=2)
    line_rank = jax.vmap(ranks_of)(named)
    scatter = (line_rank.transpose(0, 2, 1)[..., None] == slots).astype(BF16)

    def halves(values):
        return (
            lax.dynamic_slice_in_dim(values, first_col, half_cols, 1),
            lax.dynamic_slice_in_dim(values, half_cols - first_col, half_cols, 1),
        )

    own, oth = halves(routed_part)
    sh_own, sh_oth = halves(shared_part)
    blocks = (planes, width, capacity, half_cols)
    token_grad, shared_sum = combine(
        planes, own.reshape(blocks), oth.reshape(blocks), sh_own, sh_oth, scatter, grads
    )
    out_g = shared_sum[:part_rows]
    out_u = shared_sum[part_rows : 2 * part_rows]
    out_d = (
        shared_sum[2 * part_rows :]
        .reshape(part_rows, pieces, part_rows)
        .transpose(1, 0, 2)
        .reshape(hidden_cols, part_rows)
    )

    down_part = jnp.sum(out_d * out_d, axis=1)
    small = jnp.concatenate(
        [
            gate_part.reshape(experts_count, capacity),
            jnp.broadcast_to(down_part, (experts_count, hidden_cols)),
        ],
        axis=1,
    )
    small = lax.all_to_all(small, "ep", split_axis=0, concat_axis=0, tiled=True)
    back_gate, gate_norms, up_norms, shared_gate_norms, shared_up_norms = lax.psum(
        (
            small[:, :capacity],
            jnp.sum(grad_g * grad_g, axis=1),
            jnp.sum(grad_u * grad_u, axis=1),
            jnp.sum(out_g * out_g, axis=1),
            jnp.sum(out_u * out_u, axis=1),
        ),
        "tp",
    )
    down_norms = jnp.sum(small[:, capacity:], axis=0)
    token_gate = jnp.sum(jnp.where(picked, back_gate[:, :, None], 0.0), axis=1)
    gate_grad = jnp.sum(jnp.where(mine, token_gate.T[:, None, :], 0.0), axis=2) / gates
    return (
        token_grad,
        gate_grad,
        grad_g[None],
        grad_u[None],
        grad_d[None],
        out_g,
        out_u,
        out_d,
        gate_norms[None],
        up_norms[None],
        jnp.sum(grad_d * grad_d, axis=1)[None],
        shared_gate_norms,
        shared_up_norms,
        down_norms,
    )


def solution(mesh):
    placed = (
        P("ep", None),
        P("ep", None),
        P("ep", None),
        P("ep", None),
        P("ep", None, "tp"),
        P("ep", None, "tp"),
        P("ep", "tp", None),
        P(None, "tp"),
        P(None, "tp"),
        P("tp", None),
    )
    return jax.shard_map(
        functools.partial(local, plane_count(mesh)),
        mesh=mesh,
        in_specs=placed,
        out_specs=(
            P("ep", "tp"),
            P("ep", None),
            P("ep", None, "tp"),
            P("ep", None, "tp"),
            P("ep", "tp", None),
            P("ep", "tp"),
            P("ep", "tp"),
            P("tp", "ep"),
            P("ep", None),
            P("ep", None),
            P("ep", "tp"),
            P("ep"),
            P("ep"),
            P("tp"),
        ),
        check_vma=False,
    )
```

time: 591 us -> 387 us (0.65)
  waiting for transfers between devices: 228 us -> 60.9 us
  Pallas kernels: 0 us -> 84.2 us
  blocking collectives: 210 us -> 128 us
  local copies, waits for them, and re-layouts: 53.7 us -> 25.4 us
  other arithmetic: 20.9 us -> 8.37 us
  starting transfers between devices: 4.45 us -> 15.7 us
  matrix products: 56.7 us -> 49.2 us
    reduce_scatter x5 -> x0, waiting for transfers between devices: 228 us -> none  [the longest x1 97.8 us: local(): lax.psum_scatter(shared_grad_d, 'ep', scatter_dimension=1, tiled=True)]
    all_to_all x2 -> x0, blocking collectives: 89.4 us -> none  [the longest x1 79.5 us: local(): lax.all_to_all(inputs, 'ep', split_axis=0, concat_axis=0, tiled=True)]
    pallas_call x0 -> x1, Pallas kernels: none -> 84.2 us  [combine(): pl.pallas_call(functools.partial(combine_kernel, planes, width), out_shap...]
    all_to_all x1 -> x2, waiting for transfers between devices: 0.01 us -> 60.8 us  [the longest x1 60.8 us: local(): lax.all_to_all(inputs, 'ep', split_axis=0, concat_axis=0, tiled=True)]
    psum x2 -> x1, blocking collectives: 46 us -> 3.97 us  [local(): lax.psum((small[:, :capacity], jnp.sum(grad_g * grad_g, axis=1), jnp.sum(...]
    all_gather x0 -> x1, blocking collectives: none -> 38.5 us  [local(): all_ids = lax.all_gather(expert_ids, 'ep', axis=0)]
    gather x6 -> x0, local copies, waits for them, and re-layouts: 29.2 us -> none  [the longest x2 6.28 us: local(): gate_grad = back_gate[picks] / gates]
    all_to_all x1 -> x2, starting transfers between devices: 3.75 us -> 15.6 us  [the longest x1 8.52 us: local(): lax.all_to_all(inputs, 'ep', split_axis=0, concat_axis=0, tiled=True)]
  transfers between devices with their start and end apart: 8 -> 4, of which waited for: 3 -> 1; matrix products, arithmetic and copies ran while one was open for 17% -> 14% of each run, Pallas kernels for 0% -> 0%
where the time goes in v1:
time: 387 us; the launch traced here: 386 us
  blocking collectives  128 us (33%)
  Pallas kernels  84.2 us (22%)
  waiting for transfers between devices  60.9 us (16%)
  matrix products  49.2 us (13%)
  local copies, waits for them, and re-layouts  25.4 us (7%)
  starting transfers between devices  15.7 us (4%)
  between operations  14.5 us (4%)
  other arithmetic  8.37 us (2%)
    all_to_all x1, blocking collectives, local(): lax.all_to_all(scaled, 'ep', split_axis=0, concat_axis=0, tiled=True)  85.8 us
    pallas_call x1, Pallas kernels, combine(): pl.pallas_call(functools.partial(combine_kernel, planes, width), out_shap...  84.2 us
    all_to_all x1, waiting for transfers between devices, local(): lax.all_to_all(inputs, 'ep', split_axis=0, concat_axis=0, tiled=True)  60.8 us
    all_gather x1, blocking collectives, local(): all_ids = lax.all_gather(expert_ids, 'ep', axis=0)  38.5 us
    dot_general x2, matrix products, expert_backward(): hidden_cot = jnp.dot(cot_rows, w_d.T, preferred_element_type=F32)  10.6 us
    unnamed x61, local copies, waits for them, and re-layouts  10.1 us
    all_to_all x1, starting transfers between devices, local(): lax.all_to_all(inputs, 'ep', split_axis=0, concat_axis=0, tiled=True)  8.52 us
  transfers between devices with their start and end apart: 4, of which 1 were waited for; matrix products, arithmetic and copies ran while one was open for 14% of the time, Pallas kernels for 0%

profile of v1, /device:TPU:0, one launch (start us, length us, event | category | flops | bytes accessed | tf_op | source)
XLA Modules:
  0.0 386.4 jit_solution(17168176981794608647)
XLA Ops:
  8.6 3.7 convolution_convert_fusion
  12.3 8.5 %all-to-all-start.1 = ((bf16[16,96,1024]{2,1,0:T(8,128)(2,1)}), bf16[16,96,1024]{2,1,0:T(8,128)(2,1)}, u32[]{:S(2)}, u32[]{:S(2)}) async-start(bf16[16,96,1024]{2,1,0:T(8,128)(2,1)} %bitcast.91), calls=%async_computation.1 | async-start | bytes 6291456 | tf_op jit(solution)/shard_map/all_to_all | solution.py:238
  21.0 60.8 %all-to-all-done.1 = bf16[16,96,1024]{2,1,0:T(8,128)(2,1)} async-done(((bf16[16,96,1024]{2,1,0:T(8,128)(2,1)}), bf16[16,96,1024]{2,1,0:T(8,128)(2,1)}, u32[]{:S(2)}, u32[]{:S(2)}) %all-to-all-start.1) | async-done | bytes 3145760 | tf_op jit(solution)/shard_map/all_to_all | solution.py:238
  83.3 85.8 %all_to_all.36 = bf16[16,96,1024]{2,1,0:T(8,128)(2,1)} all-to-all(bf16[16,96,1024]{2,1,0:T(8,128)(2,1)S(1)} %bitcast.93), channel_id=1, replica_groups=mesh['ep'=16,'tp'=2] {'ep'}, dimensions={0} | all-to-all | bytes 6291456 | tf_op jit(solution)/shard_map/all_to_all | solution.py:239
  169.1 1.2 copy-done.2
  173.1 2.1 copy.75
  175.1 2.6 reshape.101
  177.7 3.0 multiply_convert_fusion.5
  180.7 1.4 fusion.2
  182.2 2.3 copy.65
  184.4 1.4 fusion.1
  185.9 2.3 copy.64
  188.2 38.5 %all-gather = s32[4096,4]{0,1:T(4,128)S(1)} all-gather(s32[256,4]{0,1:T(4,128)S(1)} %copy-done.18), channel_id=2, replica_groups=mesh['ep'=16,'tp'=2] {'ep'}, dimensions={0}, use_global_device_ids=true | all-gather | bytes 69632 | tf_op jit(solution)/shard_map/all_gather | solution.py:212
  227.8 1.1 constant_dynamic-slice_fusion
  229.8 1.7 pad_maximum_fusion.grads
  231.7 1.5 fusion.3.scatter
  233.3 5.9 %fusion.10 = f32[1536,256]{0,1:T(8,128)} fusion(bf16[1536,2048]{1,0:T(8,128)(2,1)} %all-gather.6.cloned.1.call-done, bf16[1,2048,256]{2,1,0:T(8,128)(2,1)S(1)} %copy-done), kind=kOutput, calls=%fused_computation.33 | convolution fusion | flops 1610612736 | bytes 8912896 | tf_op jit(solution)/shard_map/dot_general | solution.py:21
  239.2 3.0 fusion.13
  242.2 7.6 %multiply_reduce_fusion.3 = (f32[1536]{0:T(1024)S(1)}, bf16[1536,256]{0,1:T(8,128)(2,1)}, bf16[1536,256]{0,1:T(8,128)(2,1)S(1)}, bf16[1536,256]{0,1:T(8,128)(2,1)}) fusion(f32[1536,256]{0,1:T(8,128)} %fusion.13, f32[1536,256]{0,1:T(8,128)} %fusion.10, bf16[1536,2048]{1,0:T(8,128)(2,1)} %all-gather.4.cloned.1.call-done, bf16[1,256,2048]{2,1,0:T(8,128)(2,1)} %param.16), kind=kOutput, calls=%fused_computation.18 | convolution fusion | flops 1617689088 | bytes 12851200 | tf_op jit(solution)/shard_map/dot_general | solution.py:25
  249.8 1.9 fusion.8
  251.7 3.0 add_convert_fusion
  254.7 3.3 constant_dynamic-slice_fusion.2
  258.0 84.2 %combine.1 = (bf16[256,1024]{1,0:T(8,128)(2,1)}, f32[384,256]{1,0:T(8,128)}) custom-call(bf16[4,4,96,1024]{3,2,1,0:T(8,128)(2,1)} %bitcast.95, bf16[4,4,96,1024]{3,2,1,0:T(8,128)(2,1)} %bitcast.94, bf16[256,1024]{1,0:T(8,128)(2,1)} %get-tuple-element.104.sh_own, bf16[256,1024]{1,0:T(8,128)(2,1)} %get-tuple-element.103.sh_oth, ...), custom_call_target="tpu_custom_call" | custom-call | tf_op jit(solution)/shard_map/combine/pallas_call | solution.py:168
  342.2 1.8 multiply_reduce_fusion.4
  345.1 7.1 %all-to-all-start.2 = ((f32[16,1,352]{2,1,0:T(1,128)}), f32[16,1,352]{2,1,0:T(1,128)S(1)}, u32[]{:S(2)}, u32[]{:S(2)}) async-start(f32[16,1,352]{2,1,0:T(1,128)} %all_to_all.30), calls=%async_computation.2 | async-start | bytes 49152 | tf_op jit(solution)/shard_map/all_to_all | solution.py:297
  352.2 4.7 %multiply_reduce_fusion.2 = (f32[2048]{0:T(1024)S(1)}, f32[2048,256]{0,1:T(8,128)S(1)}) fusion(bf16[1536,256]{0,1:T(8,128)(2,1)S(1)} %copy-done.12, bf16[1536,2048]{1,0:T(8,128)(2,1)} %all-gather.6.cloned.1.call-done), kind=kOutput, calls=%fused_computation.13 | convolution fusion | flops 1611659264 | bytes 9183232 | tf_op jit(solution)/shard_map/dot_general | solution.py:30
  357.0 6.0 %multiply_reduce_fusion.1 = (f32[2048]{0:T(1024)S(1)}, f32[2048,256]{0,1:T(8,128)}) fusion(bf16[1536,256]{0,1:T(8,128)(2,1)S(1)} %copy-done.15, bf16[1536,2048]{1,0:T(8,128)(2,1)} %all-gather.6.cloned.1.call-done), kind=kOutput, calls=%fused_computation.12 | convolution fusion | flops 1611659264 | bytes 9183232 | tf_op jit(solution)/shard_map/dot_general | solution.py:31
  363.1 3.7 multiply_reduce_fusion
  366.8 2.9 copy.70
  369.7 1.8 copy.69
  372.8 4.0 %all-reduce = (f32[16,96]{1,0:T(8,128)S(1)}, f32[1,2048]{1,0:T(1,128)}, f32[1,2048]{1,0:T(1,128)}, f32[128]{0:T(128)}, f32[128]{0:T(128)}) all-reduce(f32[16,96]{1,0:T(8,128)S(1)} %slice.20, f32[1,2048]{1,0:T(1,128)S(1)} %bitcast.109, f32[1,2048]{1,0:T(1,128)S(1)} %bitcast.110, ...), channel_id=1, replica_groups=mesh['ep'=16,'tp'=2] {'tp'}, use_global_device_ids=true, to_apply=%region_6.7 | all-reduce | flops 5888 | bytes 47104 | tf_op jit(solution)/shard_map/psum | solution.py:298
  377.7 1.9 copy.81
  (97 shorter events, 11.4 us)
Async XLA Ops:
  7.2 226.1 %copy-start = (bf16[1,2048,256]{2,1,0:T(8,128)(2,1)S(1)}, bf16[1,2048,256]{2,1,0:T(8,128)(2,1)}, u32[]{:S(2)}) copy-start(bf16[1,2048,256]{2,1,0:T(8,128)(2,1)} %param.14) | copy-start | bytes 3145732
  7.2 0.9 copy-start.23
  12.3 8.6 %copy-start.17 = (s32[256,4]{0,1:T(4,128)S(1)}, s32[256,4]{0,1:T(4,128)}, u32[]{:S(2)}) copy-start(s32[256,4]{0,1:T(4,128)} %param.11) | copy-start | bytes 12292
  12.3 8.6 %copy-start.20 = (f32[256,4]{0,1:T(4,128)S(1)}, f32[256,4]{0,1:T(4,128)}, u32[]{:S(2)}) copy-start(f32[256,4]{0,1:T(4,128)} %param.12) | copy-start | bytes 12292
  12.3 69.5 %all-to-all-start.1 = ((bf16[16,96,1024]{2,1,0:T(8,128)(2,1)}), bf16[16,96,1024]{2,1,0:T(8,128)(2,1)}, u32[]{:S(2)}, u32[]{:S(2)}) async-start(bf16[16,96,1024]{2,1,0:T(8,128)(2,1)} %bitcast.91), calls=%async_computation.1 | async-start | bytes 6291456 | tf_op jit(solution)/shard_map/all_to_all | solution.py:238
  20.9 61.4 %copy-start.9 = (bf16[256,2048]{1,0:T(8,128)(2,1)S(1)}, bf16[256,2048]{1,0:T(8,128)(2,1)}, u32[]{:S(2)}) copy-start(bf16[256,2048]{1,0:T(8,128)(2,1)} %param.13) | copy-start | bytes 3145732
  20.9 212.4 %all-gather.6.cloned.1.call-start = ((), (), s32[]{:S(2)}) async-start(), calls=%async_computation.4 | async-start | bytes 9437184 | tf_op jit(solution)/shard_map/all_gather | solution.py:242
  81.8 160.4 %all-gather.4.cloned.1.call-start = ((), (), s32[]{:S(2)}) async-start(), calls=%async_computation.3 | async-start | bytes 9437184 | tf_op jit(solution)/shard_map/all_gather | solution.py:243
  169.1 1.2 copy-start.2
  169.1 1.5 copy-start.3
  170.6 1.2 copy-start.4
  170.6 1.7 copy-start.10
  172.3 0.7 copy-start.14
  180.7 3.7 copy-start.16
  184.4 3.7 copy-start.18
  188.2 39.1 %copy-start.5 = (bf16[2048,256]{1,0:T(8,128)(2,1)S(1)}, bf16[2048,256]{1,0:T(8,128)(2,1)}, u32[]{:S(2)}) copy-start(bf16[2048,256]{1,0:T(8,128)(2,1)} %param.18) | copy-start | bytes 3145732
  227.3 1.6 copy-start.8
  227.8 1.7 copy-start.6
  227.8 2.0 copy-start.7
  229.8 1.7 copy-start.24
  233.3 5.9 %copy-start.13 = (bf16[1,2048,256]{2,1,0:T(8,128)(2,1)S(1)}, bf16[1,2048,256]{2,1,0:T(8,128)(2,1)}, u32[]{:S(2)}) copy-start(bf16[1,2048,256]{2,1,0:T(8,128)(2,1)} %param.15) | copy-start | bytes 3145732
  233.3 5.9 %copy-start.22 = (bf16[1536,2048]{1,0:T(8,128)(2,1)S(1)}, bf16[1536,2048]{1,0:T(8,128)(2,1)}, u32[]{:S(2)}) copy-start(bf16[1536,2048]{1,0:T(8,128)(2,1)} %all-gather.6.cloned.1.call-done) | copy-start | bytes 18874372
  249.8 1.9 copy-start.11
  258.0 94.2 %copy-start.12 = (bf16[1536,256]{0,1:T(8,128)(2,1)S(1)}, bf16[1536,256]{0,1:T(8,128)(2,1)}, u32[]{:S(2)}) copy-start(bf16[1536,256]{0,1:T(8,128)(2,1)} %copy-done.11) | copy-start | bytes 2359300
  345.1 27.1 %all-to-all-start.2 = ((f32[16,1,352]{2,1,0:T(1,128)}), f32[16,1,352]{2,1,0:T(1,128)S(1)}, u32[]{:S(2)}, u32[]{:S(2)}) async-start(f32[16,1,352]{2,1,0:T(1,128)} %all_to_all.30), calls=%async_computation.2 | async-start | bytes 49152 | tf_op jit(solution)/shard_map/all_to_all | solution.py:297
  352.2 4.8 %copy-start.15 = (bf16[1536,256]{0,1:T(8,128)(2,1)S(1)}, bf16[1536,256]{0,1:T(8,128)(2,1)}, u32[]{:S(2)}) copy-start(bf16[1536,256]{0,1:T(8,128)(2,1)} %get-tuple-element.102) | copy-start | bytes 2359300
  352.2 10.8 %slice-start = ((s8[6291456]{0:T(1024)(128)(4,1)}), s8[4194304]{0:T(1024)(128)(4,1)S(1)}, s32[]{:S(2)}) async-start(s8[6291456]{0:T(1024)(128)(4,1)} %bitcast.112), calls=%async_computation.5 | async-start | bytes 8388608
  357.0 6.1 %slice-start.1 = ((s8[6291456]{0:T(1024)(128)(4,1)}), s8[2097152]{0:T(1024)(128)(4,1)S(1)}, s32[]{:S(2)}) async-start(s8[6291456]{0:T(1024)(128)(4,1)} %bitcast.112), calls=%async_computation.6 | async-start | bytes 4194304
  357.0 6.1 %copy-start.25 = (bf16[1536,256]{0,1:T(8,128)(2,1)S(1)}, bf16[1536,256]{0,1:T(8,128)(2,1)}, u32[]{:S(2)}) copy-start(bf16[1536,256]{0,1:T(8,128)(2,1)} %get-tuple-element.98) | copy-start | bytes 2359300
  369.6 9.9 %copy-start.1 = (bf16[1,2048,256]{2,1,0:T(8,128)(2,1)S(1)}, bf16[1,2048,256]{2,1,0:T(8,128)(2,1)}, u32[]{:S(2)}) copy-start(bf16[1,2048,256]{2,1,0:T(8,128)(2,1)} %param.14) | copy-start | bytes 3145732
  369.6 7.4 %copy-start.19 = (s32[256,4]{0,1:T(4,128)S(1)}, s32[256,4]{0,1:T(4,128)}, u32[]{:S(2)}) copy-start(s32[256,4]{0,1:T(4,128)} %param.11) | copy-start | bytes 12292
  369.6 7.5 %copy-start.21 = (f32[256,4]{0,1:T(4,128)S(1)}, f32[256,4]{0,1:T(4,128)}, u32[]{:S(2)}) copy-start(f32[256,4]{0,1:T(4,128)} %param.12) | copy-start | bytes 12292
Sparse Core Ops, SparseCore 0:
  81.9 26.2 all-gather.5
  169.2 15.1 all-gather.3

commit v2 on v1

--- a/solution.py
+++ b/solution.py
@@ -198,6 +198,236 @@
     )(own, oth, sh_own, sh_oth, scatter, grads)
 
 
+def dispatch_kernel(
+    planes, width, cap,
+    x, table,
+    tok_out, cot_out, line_table,
+    held, ready,
+    table_sem, line_sem, plane_sem, own_sem, pair_sem,
+):
+    me, core = lax.axis_index("ep"), lax.axis_index("tp")
+    z, q = me // width, me % width
+    cols = x.shape[1] // 2
+    mine = pl.ds(pl.multiple_of(core * cols, cols), cols)
+    outs = (tok_out, cot_out)
+
+    table_copies = []
+    for step in range(1, planes):
+        peer = (z + step) % planes * width + q
+        copy = copy_to(
+            table, line_table.at[z], table_sem.at[0, step - 1], table_sem.at[1, step - 1], peer, core
+        )
+        copy.start()
+        table_copies.append(copy)
+    line_table[z] = table[...]
+
+    def hop(step, way):
+        block = z - (step - 1) if way == 0 else z + (step - 1)
+        there = z + 1 if way == 0 else z - 1
+        valid = (block >= 0) & (block < planes) & (there >= 0) & (there < planes)
+        block, there = jnp.clip(block, 0, planes - 1), jnp.clip(there, 0, planes - 1)
+        source = x if step == 1 else held.at[block]
+        copy = copy_to(
+            source,
+            held.at[block],
+            line_sem.at[0, step - 1, way],
+            line_sem.at[1, step - 1, way],
+            there * width + q,
+            core,
+        )
+        return valid, copy
+
+    def arrival(step, way):
+        block = z - step if way == 0 else z + step
+        valid = (block >= 0) & (block < planes)
+        block = jnp.clip(block, 0, planes - 1)
+        copy = copy_to(
+            held.at[block],
+            held.at[block],
+            line_sem.at[0, step - 1, way],
+            line_sem.at[1, step - 1, way],
+            me,
+            1 - core,
+        )
+        return valid, block, copy
+
+    def send_step(step):
+        for way in range(2):
+            valid, copy = hop(step, way)
+
+            @pl.when(valid)
+            def _(copy=copy):
+                copy.start()
+
+    def plane_copy(block, d, part, from_q, to_q):
+        return copy_to(
+            ready.at[block, d, :, pl.ds(part * cols, cols)],
+            outs[part].at[block, from_q, :, mine],
+            plane_sem.at[0, block, d, part],
+            plane_sem.at[1, block, d, part],
+            z * width + to_q,
+            core,
+        )
+
+    def own_copy(block, part):
+        return pltpu.make_async_copy(
+            ready.at[block, 0, :, pl.ds(part * cols, cols)],
+            outs[part].at[block, q, :, mine],
+            own_sem.at[block, part],
+        )
+
+    def pair_copy(block, d, part):
+        from_q = (q + width - d) % width
+        return copy_to(
+            outs[part].at[block, from_q, :, mine],
+            outs[part].at[block, from_q, :, mine],
+            pair_sem.at[0, block, d, part],
+            pair_sem.at[1, block, d, part],
+            me,
+            1 - core,
+        )
+
+    def select(block, source):
+        def one(index, carry):
+            d = (index + 1) % width
+            to_q = (q + d) % width
+            expert = z * width + to_q
+            ranks = line_table[block, 0, pl.ds(expert, 1), :]
+            gates = line_table[block, 1, pl.ds(expert, 1), :]
+            slots = lax.broadcasted_iota(jnp.int32, (cap, ranks.shape[1]), 0).astype(F32)
+            hit = slots == ranks
+            gate = jnp.sum(jnp.where(hit, gates, 0.0), axis=1, keepdims=True)
+            rows = jnp.dot(
+                jnp.where(hit, 1.0, 0.0).astype(BF16), source[...], preferred_element_type=F32
+            )
+            ready[block, d, :, :cols] = rows[:, :cols].astype(BF16)
+            ready[block, d, :, cols:] = (rows[:, cols:] * gate).astype(BF16)
+
+            @pl.when(d > 0)
+            def _():
+                for part in range(2):
+                    plane_copy(block, d, part, q, to_q).start()
+
+            @pl.when(d == 0)
+            def _():
+                for part in range(2):
+                    own_copy(block, part).start()
+
+            return carry
+
+        lax.fori_loop(0, width, one, 0)
+
+    def pass_on(block):
+        for part in range(2):
+            own_copy(block, part).wait()
+            pair_copy(block, 0, part).start()
+
+        def one(d, carry):
+            for part in range(2):
+                plane_copy(block, d, part, (q + width - d) % width, (q + d) % width).wait_recv()
+                pair_copy(block, d, part).start()
+            return carry
+
+        lax.fori_loop(1, width, one, 0)
+
+    send_step(1)
+    select(z, x)
+    for copy in table_copies:
+        copy.wait_recv()
+    for step in range(1, planes):
+        for way in range(2):
+            valid, block, copy = arrival(step, way)
+
+            @pl.when(valid)
+            def _(copy=copy):
+                copy.wait_recv()
+
+            if step < planes - 1:
+                onward, hop_copy = hop(step + 1, way)
+
+                @pl.when(onward)
+                def _(hop_copy=hop_copy):
+                    hop_copy.start()
+
+            @pl.when(valid)
+            def _(block=block):
+                select(block, held.at[block])
+
+        if step == 1:
+            pass_on(z)
+        else:
+            for way in range(2):
+                valid, block, copy = arrival(step - 1, way)
+
+                @pl.when(valid)
+                def _(block=block):
+                    pass_on(block)
+
+    if planes == 1:
+        pass_on(z)
+    else:
+        for way in range(2):
+            valid, block, copy = arrival(planes - 1, way)
+
+            @pl.when(valid)
+            def _(block=block):
+                pass_on(block)
+
+    for copy in table_copies:
+        copy.wait_send()
+    for step in range(1, planes):
+        for way in range(2):
+            valid, copy = hop(step, way)
+
+            @pl.when(valid)
+            def _(copy=copy):
+                copy.wait_send()
+
+    def drain(block, carry):
+        def one(d, inner):
+            for part in range(2):
+                pair_copy(block, d, part).wait()
+
+                @pl.when(d > 0)
+                def _():
+                    plane_copy(block, d, part, q, (q + d) % width).wait_send()
+
+            return inner
+
+        return lax.fori_loop(0, width, one, carry)
+
+    lax.fori_loop(0, planes, drain, 0)
+
+
+def dispatch(planes, x, table, cap):
+    experts_count, rows = table.shape[1:]
+    width = experts_count // planes
+    model = x.shape[1]
+    vmem = pl.BlockSpec(memory_space=pltpu.VMEM)
+    anywhere = pl.BlockSpec(memory_space=pl.ANY)
+    landed = jax.ShapeDtypeStruct((planes, width, cap, model), BF16)
+    far = max(planes - 1, 1)
+    return pl.pallas_call(
+        functools.partial(dispatch_kernel, planes, width, cap),
+        out_shape=(landed, landed, jax.ShapeDtypeStruct((planes,) + table.shape, F32)),
+        in_specs=[vmem, vmem],
+        out_specs=(anywhere, anywhere, vmem),
+        scratch_shapes=[
+            pltpu.VMEM((planes, rows, model), BF16),
+            pltpu.VMEM((planes, width, cap, model), BF16),
+            pltpu.SemaphoreType.DMA((2, far)),
+            pltpu.SemaphoreType.DMA((2, far, 2)),
+            pltpu.SemaphoreType.DMA((2, planes, width, 2)),
+            pltpu.SemaphoreType.DMA((planes, 2)),
+            pltpu.SemaphoreType.DMA((2, planes, width, 2)),
+        ],
+        compiler_params=pltpu.CompilerParams(
+            has_side_effects=True, vmem_limit_bytes=60 * 2**20
+        ),
+        name="dispatch",
+    )(x, table)
+
+
 def local(planes, tokens, expert_ids, gates, cotangent, w_gate, w_up, w_down, sh_gate, sh_up, sh_down):
     experts_count = lax.axis_size("ep")
     width = experts_count // planes
@@ -209,10 +439,6 @@
     half_cols = model_width // lax.axis_size("tp")
     first_col = core * half_cols
 
-    all_ids = lax.all_gather(expert_ids, "ep", axis=0)
-    line_ids = lax.dynamic_index_in_dim(
-        all_ids.reshape(planes, width, tok_rows, top_count), q, 1, keepdims=False
-    )
     lanes = jnp.arange(experts_count, dtype=jnp.int32)
     earlier = jnp.tril(jnp.ones((tok_rows, tok_rows), BF16), -1)
 
@@ -225,23 +451,17 @@
     gate_of = jnp.sum(jnp.where(mine, gates[:, :, None], 0.0), axis=1)
     slots = jnp.arange(capacity, dtype=jnp.int32)
     picked = rank.T[:, None, :] == slots[None, :, None]
-    slot_gate = jnp.sum(jnp.where(picked, gate_of.T[:, None, :], 0.0), axis=2)
-    picked_rows = picked.astype(BF16).reshape(experts_count * capacity, tok_rows)
-
-    tok_half = lax.dynamic_slice_in_dim(tokens, first_col, half_cols, 1)
-    cot_half = lax.dynamic_slice_in_dim(cotangent, first_col, half_cols, 1)
-    inputs = jnp.dot(picked_rows, tok_half, preferred_element_type=F32).astype(BF16)
-    scaled = (
-        jnp.dot(picked_rows, cot_half, preferred_element_type=F32) * slot_gate.reshape(-1, 1)
-    ).astype(BF16)
-    part_in, part_cot = (
-        lax.all_to_all(inputs, "ep", split_axis=0, concat_axis=0, tiled=True),
-        lax.all_to_all(scaled, "ep", split_axis=0, concat_axis=0, tiled=True),
-    )
-    got_in, got_cot = (
-        lax.all_gather(part_in, "tp", axis=1, tiled=True),
-        lax.all_gather(part_cot, "tp", axis=1, tiled=True),
-    )
+    table = jnp.stack([rank.T.astype(F32), gate_of.T])
+    x = jnp.concatenate(
+        [
+            lax.dynamic_slice_in_dim(tokens, first_col, half_cols, 1),
+            lax.dynamic_slice_in_dim(cotangent, first_col, half_cols, 1),
+        ],
+        axis=1,
+    )
+    got_in, got_cot, line_table = dispatch(planes, x, table, capacity)
+    got_in = got_in.reshape(experts_count * capacity, model_width)
+    got_cot = got_cot.reshape(experts_count * capacity, model_width)
     shared_g, shared_u, shared_d, shared_part, unused = expert_backward(
         tokens, cotangent, sh_gate, sh_up, sh_down
     )
@@ -260,10 +480,8 @@
     )
 
     senders = z * width + (q - jnp.arange(width, dtype=jnp.int32)) % width
-    named = line_ids[:, :, :, None] == senders
-    named = jnp.any(named, axis=2)
-    line_rank = jax.vmap(ranks_of)(named)
-    scatter = (line_rank.transpose(0, 2, 1)[..., None] == slots).astype(BF16)
+    line_rank = line_table[:, 0][:, senders]
+    scatter = (line_rank[..., None] == slots.astype(F32)).astype(BF16)
 
     def halves(values):
         return (

time: 387 us -> 281 us (0.73)
  blocking collectives: 128 us -> 3.97 us
  Pallas kernels: 84.2 us -> 193 us
  waiting for transfers between devices: 60.9 us -> 0.01 us
  between operations: 14.5 us -> 1.06 us
  starting transfers between devices: 15.7 us -> 7.14 us
  matrix products: 49.2 us -> 40.7 us
    pallas_call x0 -> x1, Pallas kernels: none -> 108 us  [dispatch(): pl.pallas_call(functools.partial(dispatch_kernel, planes, width, cap), ou...]
    all_to_all x1 -> x0, blocking collectives: 85.8 us -> none  [local(): lax.all_to_all(scaled, 'ep', split_axis=0, concat_axis=0, tiled=True)]
    all_to_all x1 -> x0, waiting for transfers between devices: 60.8 us -> none  [local(): lax.all_to_all(inputs, 'ep', split_axis=0, concat_axis=0, tiled=True)]
    all_gather x1 -> x0, blocking collectives: 38.5 us -> none  [local(): all_ids = lax.all_gather(expert_ids, 'ep', axis=0)]
    all_to_all x1 -> x0, starting transfers between devices: 8.52 us -> none  [local(): lax.all_to_all(inputs, 'ep', split_axis=0, concat_axis=0, tiled=True)]
    dot_general x2, matrix products: 10.6 us -> 4.18 us  [expert_backward(): hidden_cot = jnp.dot(cot_rows, w_d.T, preferred_element_type=F32)]
    dot_general x2 -> x0, matrix products: 4.68 us -> none  [the longest x1 3.69 us: local(): jnp.dot(picked_rows, tok_half, preferred_element_type=F32).astype(BF16)]
    unnamed x61 -> x59, local copies, waits for them, and re-layouts: 10.1 us -> 7.67 us
  transfers between devices with their start and end apart: 4 -> 1, of which waited for: 1 -> 0; matrix products, arithmetic and copies ran while one was open for 14% -> 7% of each run, Pallas kernels for 0% -> 0%
where the time goes in v2:
time: 281 us
  Pallas kernels  193 us (69%)
  matrix products  40.7 us (14%)
  local copies, waits for them, and re-layouts  25.3 us (9%)
  other arithmetic  9.16 us (3%)
  starting transfers between devices  7.14 us (3%)
  blocking collectives  3.97 us (1%)
    pallas_call x1, Pallas kernels, dispatch(): pl.pallas_call(functools.partial(dispatch_kernel, planes, width, cap), ou...  108 us
    pallas_call x1, Pallas kernels, combine(): pl.pallas_call(functools.partial(combine_kernel, planes, width), out_shap...  85.6 us
    unnamed x59, local copies, waits for them, and re-layouts  7.67 us
    dot_general x2, matrix products, expert_backward(): grad_u = lax.dot_general(inputs, d_up, contract, preferred_element_type=F32)  7.48 us
    all_to_all x1, starting transfers between devices, local(): small = lax.all_to_all(small, 'ep', split_axis=0, concat_axis=0, tiled=True)  7.14 us
    dot_general x2, matrix products, expert_backward(): gate_pre = jnp.dot(inputs, w_g, preferred_element_type=F32)  6.91 us
    dot_general x2, matrix products, expert_backward(): lax.dot_general(inputs, d_gate, contract, preferred_element_type=F32)  6.17 us
    dynamic_slice x2, local copies, waits for them, and re-layouts, halves(): lax.dynamic_slice_in_dim(values, half_cols - first_col, half_cols, 1)  5.78 us
  transfers between devices with their start and end apart: 1, of which 0 were waited for; matrix products, arithmetic and copies ran while one was open for 7% of the time, Pallas kernels for 0%

profile of v2, /device:TPU:0, one launch (start us, length us, event | category | flops | bytes accessed | tf_op | source)
XLA Modules:
  0.0 280.8 jit_solution(4747929288751229235)
XLA Ops:
  1.2 2.1 fusion.30
  5.1 1.4 fusion.1
  6.5 1.8 fusion.31
  8.9 1.1 copy.76
  10.0 1.5 reshape.133
  11.5 0.8 constant_dynamic-slice_fusion.5
  12.3 1.4 fusion.2
  13.8 2.4 copy.66
  16.2 2.3 copy.65
  18.4 2.7 fusion
  21.7 2.4 constant_dynamic-slice_fusion
  24.2 1.1 pad_maximum_fusion.1.x
  25.2 107.8 %dispatch.1 = (bf16[4,4,96,2048]{3,2,1,0:T(8,128)(2,1)}, bf16[4,4,96,2048]{3,2,1,0:T(8,128)(2,1)}, f32[4,2,16,256]{3,2,1,0:T(8,128)}) custom-call(bf16[256,2048]{1,0:T(8,128)(2,1)} %pad_maximum_fusion.1.x, f32[2,16,256]{2,1,0:T(8,128)} %pad_maximum_fusion.2.table), custom_call_target="tpu_custom_call" | custom-call | tf_op jit(solution)/shard_map/dispatch/pallas_call | solution.py:410
  133.0 0.8 slice_bitcast_fusion
  134.5 4.8 %fusion.8 = f32[1536,256]{0,1:T(8,128)S(1)} fusion(bf16[1536,2048]{1,0:T(8,128)(2,1)} %bitcast.109, bf16[1,2048,256]{2,1,0:T(8,128)(2,1)S(1)} %copy-done), kind=kOutput, calls=%fused_computation.28 | convolution fusion | flops 1610612736 | bytes 8912896 | tf_op jit(solution)/shard_map/dot_general | solution.py:21
  139.4 1.9 fusion.11
  141.7 3.7 %multiply_reduce_fusion.3 = (f32[1536]{0:T(1024)S(1)}, bf16[1536,256]{0,1:T(8,128)(2,1)}, bf16[1536,256]{0,1:T(8,128)(2,1)S(1)}, bf16[1536,256]{0,1:T(8,128)(2,1)}) fusion(f32[1536,256]{0,1:T(8,128)S(1)} %fusion.11, f32[1536,256]{0,1:T(8,128)S(1)} %fusion.8, bf16[1536,2048]{1,0:T(8,128)(2,1)S(1)} %bitcast.105, bf16[1,256,2048]{2,1,0:T(8,128)(2,1)S(1)} %copy-done.21), kind=kOutput, calls=%fused_computation.15 | convolution fusion | flops 1617689088 | bytes 12851200 | tf_op jit(solution)/shard_map/dot_general | solution.py:25
  146.2 1.9 fusion.6
  148.0 3.0 %add_convert_fusion = bf16[1536,2048]{1,0:T(8,128)(2,1)S(1)} fusion(f32[1536,2048]{1,0:T(8,128)S(1)} %fusion.6, bf16[1536,256]{0,1:T(8,128)(2,1)} %get-tuple-element.108, bf16[1,2048,256]{2,1,0:T(8,128)(2,1)S(1)} %copy-done.13), kind=kOutput, calls=%fused_computation.1 | convolution fusion | flops 1616904192 | bytes 20709376 | tf_op jit(solution)/shard_map/dot_general | solution.py:33
  151.1 3.3 %constant_dynamic-slice_fusion.2 = (bf16[1536,1024]{1,0:T(8,128)(2,1)}, bf16[1536,1024]{1,0:T(8,128)(2,1)}) fusion(bf16[1536,2048]{1,0:T(8,128)(2,1)S(1)} %add_convert_fusion, s32[]{:T(128)S(6)} %select_n.69, s32[]{:T(128)S(6)} %select_n.65), kind=kLoop, calls=%fused_computation.66 | loop fusion | bytes 12582920 | tf_op jit(solution)/shard_map/dynamic_slice | solution.py:489
  154.4 1.6 compare_convert_fusion.scatter
  156.0 1.8 pad_maximum_fusion.grads
  157.8 85.6 %combine.1 = (bf16[256,1024]{1,0:T(8,128)(2,1)}, f32[384,256]{1,0:T(8,128)}) custom-call(bf16[4,4,96,1024]{3,2,1,0:T(8,128)(2,1)} %bitcast.86, bf16[4,4,96,1024]{3,2,1,0:T(8,128)(2,1)} %bitcast.85, bf16[256,1024]{1,0:T(8,128)(2,1)} %get-tuple-element.110.sh_own, bf16[256,1024]{1,0:T(8,128)(2,1)} %get-tuple-element.109.sh_oth, ...), custom_call_target="tpu_custom_call" | custom-call | tf_op jit(solution)/shard_map/combine/pallas_call | solution.py:168
  243.4 1.8 multiply_reduce_fusion.4
  246.3 7.1 %all-to-all-start = ((f32[16,1,352]{2,1,0:T(1,128)}), f32[16,1,352]{2,1,0:T(1,128)S(1)}, u32[]{:S(2)}, u32[]{:S(2)}) async-start(f32[16,1,352]{2,1,0:T(1,128)} %all_to_all.8), calls=%async_computation | async-start | bytes 49152 | tf_op jit(solution)/shard_map/all_to_all | solution.py:515
  253.5 4.7 %multiply_reduce_fusion.2 = (f32[2048]{0:T(1024)S(1)}, f32[2048,256]{0,1:T(8,128)S(1)}) fusion(bf16[1536,256]{0,1:T(8,128)(2,1)S(1)} %copy-done.12, bf16[1536,2048]{1,0:T(8,128)(2,1)} %bitcast.110), kind=kOutput, calls=%fused_computation.12 | convolution fusion | flops 1611659264 | bytes 9183232 | tf_op jit(solution)/shard_map/dot_general | solution.py:30
  258.2 6.0 %multiply_reduce_fusion.1 = (f32[2048]{0:T(1024)S(1)}, f32[2048,256]{0,1:T(8,128)}) fusion(bf16[1536,256]{0,1:T(8,128)(2,1)S(1)} %copy-done.14, bf16[1536,2048]{1,0:T(8,128)(2,1)} %bitcast.111), kind=kOutput, calls=%fused_computation.11 | convolution fusion | flops 1611659264 | bytes 9183232 | tf_op jit(solution)/shard_map/dot_general | solution.py:31
  264.3 3.7 %multiply_reduce_fusion = (f32[256]{0:T(256)}, f32[256,2048]{1,0:T(8,128)}) fusion(bf16[1536,256]{0,1:T(8,128)(2,1)S(1)} %copy-done.22, bf16[1536,2048]{1,0:T(8,128)(2,1)S(1)} %bitcast.108), kind=kOutput, calls=%fused_computation.10 | convolution fusion | flops 1611661056 | bytes 9176064 | tf_op jit(solution)/shard_map/dot_general | solution.py:32
  268.0 2.9 %copy.71 = f32[1,2048,256]{2,1,0:T(8,128)} copy(f32[1,2048,256]{1,2,0:T(8,128)} %bitcast.92) | data formatting | bytes 4194304
  270.9 1.8 copy.70
  274.0 4.0 %all-reduce = (f32[16,96]{1,0:T(8,128)S(1)}, f32[1,2048]{1,0:T(1,128)}, f32[1,2048]{1,0:T(1,128)}, f32[128]{0:T(128)}, f32[128]{0:T(128)}) all-reduce(f32[16,96]{1,0:T(8,128)S(1)} %slice.26, f32[1,2048]{1,0:T(1,128)S(1)} %bitcast.100, f32[1,2048]{1,0:T(1,128)S(1)} %bitcast.101, ...), channel_id=1, replica_groups=mesh['ep'=16,'tp'=2] {'tp'}, use_global_device_ids=true, to_apply=%region_4.5 | all-reduce | flops 5888 | bytes 47104 | tf_op jit(solution)/shard_map/psum | solution.py:516
  278.9 1.9 copy.79
  (87 shorter events, 8.7 us)
Async XLA Ops:
  0.6 133.9 %copy-start = (bf16[1,2048,256]{2,1,0:T(8,128)(2,1)S(1)}, bf16[1,2048,256]{2,1,0:T(8,128)(2,1)}, u32[]{:S(2)}) copy-start(bf16[1,2048,256]{2,1,0:T(8,128)(2,1)} %param.14) | copy-start | bytes 3145732
  0.7 2.7 copy-start.2
  0.7 2.7 copy-start.5
  1.2 2.6 copy-start.9
  3.4 1.2 copy-start.20
  4.6 1.9 copy-start.4
  6.5 1.8 copy-start.15
  6.5 2.1 copy-start.17
  13.8 4.7 %copy-start.3 = (f32[256,2048]{1,0:T(8,128)S(1)}, f32[256,2048]{1,0:T(8,128)}, u32[]{:S(2)}) copy-start(f32[256,2048]{1,0:T(8,128)} %fusion.31) | copy-start | bytes 6291460
  21.1 3.1 %copy-start.10 = (bf16[256,1024]{1,0:T(8,128)(2,1)S(1)}, bf16[256,1024]{1,0:T(8,128)(2,1)}, u32[]{:S(2)}) copy-start(bf16[256,1024]{1,0:T(8,128)(2,1)} %constant_dynamic-slice_fusion.5) | copy-start | bytes 1572868
  134.5 4.8 %copy-start.13 = (bf16[1,2048,256]{2,1,0:T(8,128)(2,1)S(1)}, bf16[1,2048,256]{2,1,0:T(8,128)(2,1)}, u32[]{:S(2)}) copy-start(bf16[1,2048,256]{2,1,0:T(8,128)(2,1)} %param.15) | copy-start | bytes 3145732
  134.5 4.9 %copy-start.19 = (bf16[4,4,96,2048]{3,2,1,0:T(8,128)(2,1)S(1)}, bf16[4,4,96,2048]{3,2,1,0:T(8,128)(2,1)}, u32[]{:S(2)}) copy-start(bf16[4,4,96,2048]{3,2,1,0:T(8,128)(2,1)} %get-tuple-element.20) | copy-start | bytes 18874372
  134.5 6.8 %slice-start = ((s8[6291456]{0:T(1024)(128)(4,1)}), s8[4194304]{0:T(1024)(128)(4,1)S(1)}, s32[]{:S(2)}) async-start(s8[6291456]{0:T(1024)(128)(4,1)} %bitcast.103), calls=%async_computation.1 | async-start | bytes 8388608
  139.4 2.0 slice-start.1
  139.4 2.2 copy-start.21
  145.4 2.6 copy-start.11
  151.0 3.4 %copy-start.18 = (f32[96]{0:T(128)S(1)}, f32[96]{0:T(128)}, u32[]{:S(2)}) copy-start(f32[96]{0:T(128)} %iota_convert_fusion) | copy-start | bytes 1156
  151.1 5.0 %copy-start.6 = (bf16[4,4,128,256]{3,2,1,0:T(8,128)(2,1)S(1)}, bf16[4,4,128,256]{3,2,1,0:T(8,128)(2,1)}, u32[]{:S(2)}) copy-start(bf16[4,4,128,256]{3,2,1,0:T(8,128)(2,1)} %reshape.133) | copy-start | bytes 3145732
  151.1 4.9 %copy-start.7 = (bf16[2048,256]{1,0:T(8,128)(2,1)S(1)}, bf16[2048,256]{1,0:T(8,128)(2,1)}, u32[]{:S(2)}) copy-start(bf16[2048,256]{1,0:T(8,128)(2,1)} %copy.66) | copy-start | bytes 3145732
  151.1 4.9 %copy-start.8 = (bf16[2048,256]{1,0:T(8,128)(2,1)S(1)}, bf16[2048,256]{1,0:T(8,128)(2,1)}, u32[]{:S(2)}) copy-start(bf16[2048,256]{1,0:T(8,128)(2,1)} %copy.65) | copy-start | bytes 3145732
  157.8 87.8 %copy-start.16 = (f32[16,96]{1,0:T(8,128)S(1)}, f32[16,96]{1,0:T(8,128)}, u32[]{:S(2)}) copy-start(f32[16,96]{1,0:T(8,128)} %reshape.134) | copy-start | bytes 18436
  157.8 95.6 %copy-start.12 = (bf16[1536,256]{0,1:T(8,128)(2,1)S(1)}, bf16[1536,256]{0,1:T(8,128)(2,1)}, u32[]{:S(2)}) copy-start(bf16[1536,256]{0,1:T(8,128)(2,1)} %copy-done.11) | copy-start | bytes 2359300
  246.3 27.1 %all-to-all-start = ((f32[16,1,352]{2,1,0:T(1,128)}), f32[16,1,352]{2,1,0:T(1,128)S(1)}, u32[]{:S(2)}, u32[]{:S(2)}) async-start(f32[16,1,352]{2,1,0:T(1,128)} %all_to_all.8), calls=%async_computation | async-start | bytes 49152 | tf_op jit(solution)/shard_map/all_to_all | solution.py:515
  253.4 4.8 %copy-start.14 = (bf16[1536,256]{0,1:T(8,128)(2,1)S(1)}, bf16[1536,256]{0,1:T(8,128)(2,1)}, u32[]{:S(2)}) copy-start(bf16[1536,256]{0,1:T(8,128)(2,1)} %get-tuple-element.108) | copy-start | bytes 2359300
  253.4 10.8 %slice-start.2 = ((s8[6291456]{0:T(1024)(128)(4,1)}), s8[4194304]{0:T(1024)(128)(4,1)S(1)}, s32[]{:S(2)}) async-start(s8[6291456]{0:T(1024)(128)(4,1)} %bitcast.106), calls=%async_computation.3 | async-start | bytes 8388608
  258.2 6.1 %slice-start.3 = ((s8[6291456]{0:T(1024)(128)(4,1)}), s8[2097152]{0:T(1024)(128)(4,1)S(1)}, s32[]{:S(2)}) async-start(s8[6291456]{0:T(1024)(128)(4,1)} %bitcast.106), calls=%async_computation.4 | async-start | bytes 4194304
  258.2 6.1 %copy-start.22 = (bf16[1536,256]{0,1:T(8,128)(2,1)S(1)}, bf16[1536,256]{0,1:T(8,128)(2,1)}, u32[]{:S(2)}) copy-start(bf16[1536,256]{0,1:T(8,128)(2,1)} %get-tuple-element.104) | copy-start | bytes 2359300
  270.9 9.9 %copy-start.1 = (bf16[1,2048,256]{2,1,0:T(8,128)(2,1)S(1)}, bf16[1,2048,256]{2,1,0:T(8,128)(2,1)}, u32[]{:S(2)}) copy-start(bf16[1,2048,256]{2,1,0:T(8,128)(2,1)} %param.14) | copy-start | bytes 3145732

commit v3 on v2

--- a/solution.py
+++ b/solution.py
@@ -200,8 +200,8 @@
 
 def dispatch_kernel(
     planes, width, cap,
-    x, table,
-    tok_out, cot_out, line_table,
+    x, table, tokens, cotangent, w_g, w_u, w_d,
+    tok_out, cot_out, line_table, grads, sh_part,
     held, ready,
     table_sem, line_sem, plane_sem, own_sem, pair_sem,
 ):
@@ -330,8 +330,46 @@
 
         lax.fori_loop(1, width, one, 0)
 
+    def shared_expert():
+        gate_pre = jnp.dot(tokens[...], w_g[...], preferred_element_type=F32)
+        up_pre = jnp.dot(tokens[...], w_u[...], preferred_element_type=F32)
+        active, slope = silu_parts(gate_pre)
+        hidden = (active * up_pre).astype(BF16)
+        last, first = (((1,), (1,)), ((), ())), (((0,), (0,)), ((), ()))
+        hidden_cot = lax.dot_general(cotangent[...], w_d[...], last, preferred_element_type=F32)
+        d_gate = (hidden_cot * up_pre * slope).astype(BF16)
+        d_up = (hidden_cot * active).astype(BF16)
+        part_rows = grads.shape[2] // 3
+        pieces = grads.shape[3] // part_rows
+        block = max(part_rows, 128)
+
+        def one(index, carry):
+            at = pl.ds(pl.multiple_of(index * block, block), block)
+            rows = lax.dot_general(d_gate, w_g[at, :], last, preferred_element_type=F32)
+            rows = rows + lax.dot_general(d_up, w_u[at, :], last, preferred_element_type=F32)
+            sh_part[:, at] = rows.astype(BF16)
+            toks = tokens[:, at]
+            grad_g = lax.dot_general(toks, d_gate, first, preferred_element_type=F32).astype(BF16)
+            grad_u = lax.dot_general(toks, d_up, first, preferred_element_type=F32).astype(BF16)
+            grad_d = lax.dot_general(
+                hidden, cotangent[:, at], first, preferred_element_type=F32
+            ).astype(BF16)
+            for i in range(block // part_rows):
+                owner = index * (block // part_rows) + i
+                oz, oq = owner // width, owner % width
+                take = slice(i * part_rows, (i + 1) * part_rows)
+                grads[oz, oq, :part_rows, :] = grad_g[take, :]
+                grads[oz, oq, part_rows : 2 * part_rows, :] = grad_u[take, :]
+                for p in range(pieces):
+                    here = slice(p * part_rows, (p + 1) * part_rows)
+                    grads[oz, oq, 2 * part_rows :, here] = grad_d[here, take]
+            return carry
+
+        lax.fori_loop(0, tokens.shape[1] // block, one, 0)
+
     send_step(1)
     select(z, x)
+    shared_expert()
     for copy in table_copies:
         copy.wait_recv()
     for step in range(1, planes):
@@ -399,7 +437,7 @@
     lax.fori_loop(0, planes, drain, 0)
 
 
-def dispatch(planes, x, table, cap):
+def dispatch(planes, x, table, cap, shared):
     experts_count, rows = table.shape[1:]
     width = experts_count // planes
     model = x.shape[1]
@@ -407,11 +445,19 @@
     anywhere = pl.BlockSpec(memory_space=pl.ANY)
     landed = jax.ShapeDtypeStruct((planes, width, cap, model), BF16)
     far = max(planes - 1, 1)
+    hidden_cols = shared[2].shape[1]
+    deal = (planes, width, 3 * (model // experts_count), hidden_cols)
     return pl.pallas_call(
         functools.partial(dispatch_kernel, planes, width, cap),
-        out_shape=(landed, landed, jax.ShapeDtypeStruct((planes,) + table.shape, F32)),
-        in_specs=[vmem, vmem],
-        out_specs=(anywhere, anywhere, vmem),
+        out_shape=(
+            landed,
+            landed,
+            jax.ShapeDtypeStruct((planes,) + table.shape, F32),
+            jax.ShapeDtypeStruct(deal, BF16),
+            jax.ShapeDtypeStruct((rows, model), BF16),
+        ),
+        in_specs=[vmem] * 7,
+        out_specs=(anywhere, anywhere, vmem, vmem, vmem),
         scratch_shapes=[
             pltpu.VMEM((planes, rows, model), BF16),
             pltpu.VMEM((planes, width, cap, model), BF16),
@@ -425,7 +471,7 @@
             has_side_effects=True, vmem_limit_bytes=60 * 2**20
         ),
         name="dispatch",
-    )(x, table)
+    )(x, table, *shared)
 
 
 def local(planes, tokens, expert_ids, gates, cotangent, w_gate, w_up, w_down, sh_gate, sh_up, sh_down):
@@ -459,12 +505,10 @@
         ],
         axis=1,
     )
-    got_in, got_cot, line_table = dispatch(planes, x, table, capacity)
+    shared = (tokens, cotangent, sh_gate, sh_up, sh_down)
+    got_in, got_cot, line_table, grads, shared_part = dispatch(planes, x, table, capacity, shared)
     got_in = got_in.reshape(experts_count * capacity, model_width)
     got_cot = got_cot.reshape(experts_count * capacity, model_width)
-    shared_g, shared_u, shared_d, shared_part, unused = expert_backward(
-        tokens, cotangent, sh_gate, sh_up, sh_down
-    )
     grad_g, grad_u, grad_d, routed_part, gate_part = expert_backward(
         got_in, got_cot, w_gate[0], w_up[0], w_down[0]
     )
@@ -472,12 +516,6 @@
     part_rows = model_width // experts_count
     hidden_cols = sh_gate.shape[1]
     pieces = hidden_cols // part_rows
-    deal = (planes, width, part_rows, hidden_cols)
-    down = shared_d.astype(BF16).reshape(pieces, part_rows, experts_count, part_rows)
-    down = down.transpose(2, 1, 0, 3).reshape(deal)
-    grads = jnp.concatenate(
-        [shared_g.astype(BF16).reshape(deal), shared_u.astype(BF16).reshape(deal), down], axis=2
-    )
 
     senders = z * width + (q - jnp.arange(width, dtype=jnp.int32)) % width
     line_rank = line_table[:, 0][:, senders]

time: 281 us -> 272 us (0.968)
  local copies, waits for them, and re-layouts: 25.3 us -> 17.1 us
  Pallas kernels: 193 us -> 196 us
  matrix products: 40.7 us -> 37.8 us
    convert_element_type x2 -> x0, local copies, waits for them, and re-layouts: 4.68 us -> none  [the longest x1 2.42 us: local(): shared_u.astype(BF16).reshape(deal)]
    pallas_call x1, Pallas kernels: 108 us -> 111 us  [dispatch(): pl.pallas_call(functools.partial(dispatch_kernel, planes, width, cap), ou...]
    dot_general x2 -> x1, matrix products: 3.64 us -> 6.43 us  [expert_backward(): jnp.dot(d_gate, w_g.T, preferred_element_type=F32)]
    dot_general x2 -> x1, matrix products: 6.91 us -> 4.77 us  [expert_backward(): gate_pre = jnp.dot(inputs, w_g, preferred_element_type=F32)]
    dot_general x2 -> x1, matrix products: 6.17 us -> 4.74 us  [expert_backward(): lax.dot_general(inputs, d_gate, contract, preferred_element_type=F32)]
    dot_general x2 -> x1, matrix products: 7.48 us -> 6.05 us  [expert_backward(): grad_u = lax.dot_general(inputs, d_up, contract, preferred_element_type=F32)]
    dot_general x2 -> x1, matrix products: 5.66 us -> 6.43 us  [expert_backward(): jnp.dot(d_up, w_u.T, preferred_element_type=F32)]
    unnamed x59 -> x36, local copies, waits for them, and re-layouts: 7.67 us -> 7.08 us
where the time goes in v3:
time: 272 us
  Pallas kernels  196 us (72%)
  matrix products  37.8 us (14%)
  local copies, waits for them, and re-layouts  17.1 us (6%)
  other arithmetic  8.35 us (3%)
  starting transfers between devices  7.13 us (3%)
  blocking collectives  3.97 us (1%)
    pallas_call x1, Pallas kernels, dispatch(): pl.pallas_call(functools.partial(dispatch_kernel, planes, width, cap), ou...  111 us
    pallas_call x1, Pallas kernels, combine(): pl.pallas_call(functools.partial(combine_kernel, planes, width), out_shap...  85.6 us
    all_to_all x1, starting transfers between devices, local(): small = lax.all_to_all(small, 'ep', split_axis=0, concat_axis=0, tiled=True)  7.13 us
    unnamed x36, local copies, waits for them, and re-layouts  7.08 us
    dot_general x1, matrix products, expert_backward(): jnp.dot(d_up, w_u.T, preferred_element_type=F32)  6.43 us
    dot_general x1, matrix products, expert_backward(): jnp.dot(d_gate, w_g.T, preferred_element_type=F32)  6.43 us
    dot_general x1, matrix products, expert_backward(): grad_u = lax.dot_general(inputs, d_up, contract, preferred_element_type=F32)  6.05 us
    dynamic_slice x2, local copies, waits for them, and re-layouts, halves(): lax.dynamic_slice_in_dim(values, half_cols - first_col, half_cols, 1)  5.7 us
  transfers between devices with their start and end apart: 1, of which 0 were waited for; matrix products, arithmetic and copies ran while one was open for 7% of the time, Pallas kernels for 0%

profile of v3, /device:TPU:0, one launch (start us, length us, event | category | flops | bytes accessed | tf_op | source)
XLA Modules:
  0.0 271.7 jit_solution(2507221402837645401)
XLA Ops:
  0.8 0.8 fusion.16
  1.5 0.2 fusion.1
  1.8 0.7 select_reduce_fusion.2
  2.5 0.6 pad_maximum_fusion.1.table
  3.1 1.3 constant_dynamic-slice_fusion.4
  4.4 1.1 pad_maximum_fusion.x
  5.5 110.8 %dispatch.1 = (bf16[4,4,96,2048]{3,2,1,0:T(8,128)(2,1)}, bf16[4,4,96,2048]{3,2,1,0:T(8,128)(2,1)}, f32[4,2,16,256]{3,2,1,0:T(8,128)}, bf16[4,4,384,256]{3,2,1,0:T(8,128)(2,1)}, bf16[256,2048]{1,0:T(8,128)(2,1)}) custom-call(bf16[256,2048]{1,0:T(8,128)(2,1)} %pad_maximum_fusion.x, f32[2,16,256]{2,1,0:T(8,128)} %pad_maximum_fusion.1.table, ...), custom_call_target="tpu_custom_call" | custom-call | tf_op jit(solution)/shard_map/dispatch/pallas_call | solution.py:450
  116.3 0.8 slice_bitcast_fusion
  117.2 0.6 gather_fusion
  117.8 4.8 %fusion.4 = f32[1536,256]{0,1:T(8,128)S(1)} fusion(bf16[1536,2048]{1,0:T(8,128)(2,1)} %bitcast.77, bf16[1,2048,256]{2,1,0:T(8,128)(2,1)S(1)} %copy-done), kind=kOutput, calls=%fused_computation.19 | convolution fusion | flops 1610612736 | bytes 8912896 | tf_op jit(solution)/shard_map/dot_general | solution.py:21
  122.7 1.9 fusion.7
  124.9 3.6 %multiply_reduce_fusion.3 = (f32[1536]{0:T(1024)S(1)}, bf16[1536,256]{0,1:T(8,128)(2,1)}, bf16[1536,256]{0,1:T(8,128)(2,1)S(1)}, bf16[1536,256]{0,1:T(8,128)(2,1)}) fusion(f32[1536,256]{0,1:T(8,128)S(1)} %fusion.7, f32[1536,256]{0,1:T(8,128)S(1)} %fusion.4, bf16[1536,2048]{1,0:T(8,128)(2,1)S(1)} %bitcast.73, bf16[1,256,2048]{2,1,0:T(8,128)(2,1)S(1)} %copy-done.10), kind=kOutput, calls=%fused_computation.7 | convolution fusion | flops 1617689088 | bytes 12851200 | tf_op jit(solution)/shard_map/dot_general | solution.py:25
  128.6 6.4 %fusion.2 = f32[1536,2048]{1,0:T(8,128)} fusion(bf16[1536,256]{0,1:T(8,128)(2,1)S(1)} %get-tuple-element.111, bf16[1,2048,256]{2,1,0:T(8,128)(2,1)S(1)} %copy-done), kind=kOutput, calls=%fused_computation.17 | convolution fusion | flops 1610612736 | bytes 14417920 | tf_op jit(solution)/shard_map/dot_general | solution.py:33
  135.1 2.3 constant_dynamic-slice_fusion
  137.4 6.4 %add_convert_fusion = bf16[1536,2048]{1,0:T(8,128)(2,1)S(1)} fusion(f32[1536,2048]{1,0:T(8,128)} %fusion.2, bf16[1536,256]{0,1:T(8,128)(2,1)S(1)} %copy-done.5, bf16[1,2048,256]{2,1,0:T(8,128)(2,1)S(1)} %copy-done.4), kind=kOutput, calls=%fused_computation.1 | convolution fusion | flops 1616904192 | bytes 20709376 | tf_op jit(solution)/shard_map/dot_general | solution.py:33
  143.8 3.4 %constant_dynamic-slice_fusion.2 = (bf16[1536,1024]{1,0:T(8,128)(2,1)}, bf16[1536,1024]{1,0:T(8,128)(2,1)}) fusion(bf16[1536,2048]{1,0:T(8,128)(2,1)S(1)} %add_convert_fusion, s32[]{:T(128)S(6)} %select_n.69, s32[]{:T(128)S(6)} %select_n.65), kind=kLoop, calls=%fused_computation.51 | loop fusion | bytes 12582920 | tf_op jit(solution)/shard_map/dynamic_slice | solution.py:527
  147.2 1.6 compare_convert_fusion.scatter
  148.8 85.6 %combine.1 = (bf16[256,1024]{1,0:T(8,128)(2,1)}, f32[384,256]{1,0:T(8,128)}) custom-call(bf16[4,4,96,1024]{3,2,1,0:T(8,128)(2,1)} %bitcast.58, bf16[4,4,96,1024]{3,2,1,0:T(8,128)(2,1)} %bitcast.57, bf16[256,1024]{1,0:T(8,128)(2,1)} %get-tuple-element.114.sh_own, bf16[256,1024]{1,0:T(8,128)(2,1)} %get-tuple-element.113.sh_oth, ...), custom_call_target="tpu_custom_call" | custom-call | tf_op jit(solution)/shard_map/combine/pallas_call | solution.py:168
  234.3 1.8 multiply_reduce_fusion.4
  236.5 0.7 all_to_all.8
  237.2 7.1 %all-to-all-start = ((f32[16,1,352]{2,1,0:T(1,128)}), f32[16,1,352]{2,1,0:T(1,128)S(1)}, u32[]{:S(2)}, u32[]{:S(2)}) async-start(f32[16,1,352]{2,1,0:T(1,128)} %all_to_all.8), calls=%async_computation | async-start | bytes 49152 | tf_op jit(solution)/shard_map/all_to_all | solution.py:553
  244.4 4.7 %multiply_reduce_fusion.2 = (f32[2048]{0:T(1024)S(1)}, f32[2048,256]{0,1:T(8,128)S(1)}) fusion(bf16[1536,256]{0,1:T(8,128)(2,1)S(1)} %copy-done.3, bf16[1536,2048]{1,0:T(8,128)(2,1)} %bitcast.78), kind=kOutput, calls=%fused_computation.4 | convolution fusion | flops 1611659264 | bytes 9183232 | tf_op jit(solution)/shard_map/dot_general | solution.py:30
  249.1 6.0 %multiply_reduce_fusion.1 = (f32[2048]{0:T(1024)S(1)}, f32[2048,256]{0,1:T(8,128)}) fusion(bf16[1536,256]{0,1:T(8,128)(2,1)S(1)} %copy-done.6, bf16[1536,2048]{1,0:T(8,128)(2,1)} %bitcast.79), kind=kOutput, calls=%fused_computation.3 | convolution fusion | flops 1611659264 | bytes 9183232 | tf_op jit(solution)/shard_map/dot_general | solution.py:31
  255.2 3.7 %multiply_reduce_fusion = (f32[256]{0:T(256)}, f32[256,2048]{1,0:T(8,128)}) fusion(bf16[1536,256]{0,1:T(8,128)(2,1)S(1)} %copy-done.11, bf16[1536,2048]{1,0:T(8,128)(2,1)S(1)} %bitcast.76), kind=kOutput, calls=%fused_computation.2 | convolution fusion | flops 1611661056 | bytes 9176064 | tf_op jit(solution)/shard_map/dot_general | solution.py:32
  258.9 2.9 %copy.56 = f32[1,2048,256]{2,1,0:T(8,128)} copy(f32[1,2048,256]{1,2,0:T(8,128)} %bitcast.60) | data formatting | bytes 4194304
  261.8 1.8 copy.55
  263.6 0.7 copy.54
  264.2 0.7 slice_reduce_fusion
  264.9 4.0 %all-reduce = (f32[16,96]{1,0:T(8,128)S(1)}, f32[1,2048]{1,0:T(1,128)}, f32[1,2048]{1,0:T(1,128)}, f32[128]{0:T(128)}, f32[128]{0:T(128)}) all-reduce(f32[16,96]{1,0:T(8,128)S(1)} %slice.26, f32[1,2048]{1,0:T(1,128)S(1)} %bitcast.68, f32[1,2048]{1,0:T(1,128)S(1)} %bitcast.69, ...), channel_id=1, replica_groups=mesh['ep'=16,'tp'=2] {'tp'}, use_global_device_ids=true, to_apply=%region_4.5 | all-reduce | flops 5888 | bytes 47104 | tf_op jit(solution)/shard_map/psum | solution.py:554
  268.9 0.3 select_reduce_fusion
  269.2 0.6 div.18
  269.8 1.9 copy.61
  (51 shorter events, 1.1 us)
Async XLA Ops:
  0.6 117.1 %copy-start = (bf16[1,2048,256]{2,1,0:T(8,128)(2,1)S(1)}, bf16[1,2048,256]{2,1,0:T(8,128)(2,1)}, u32[]{:S(2)}) copy-start(bf16[1,2048,256]{2,1,0:T(8,128)(2,1)} %param.14) | copy-start | bytes 3145732
  117.8 4.8 %copy-start.4 = (bf16[1,2048,256]{2,1,0:T(8,128)(2,1)S(1)}, bf16[1,2048,256]{2,1,0:T(8,128)(2,1)}, u32[]{:S(2)}) copy-start(bf16[1,2048,256]{2,1,0:T(8,128)(2,1)} %param.15) | copy-start | bytes 3145732
  117.8 4.9 %copy-start.9 = (bf16[4,4,96,2048]{3,2,1,0:T(8,128)(2,1)S(1)}, bf16[4,4,96,2048]{3,2,1,0:T(8,128)(2,1)}, u32[]{:S(2)}) copy-start(bf16[4,4,96,2048]{3,2,1,0:T(8,128)(2,1)} %get-tuple-element.22) | copy-start | bytes 18874372
  117.8 6.8 %slice-start = ((s8[6291456]{0:T(1024)(128)(4,1)}), s8[4194304]{0:T(1024)(128)(4,1)S(1)}, s32[]{:S(2)}) async-start(s8[6291456]{0:T(1024)(128)(4,1)} %bitcast.71), calls=%async_computation.1 | async-start | bytes 8388608
  122.7 2.0 slice-start.1
  122.7 2.2 copy-start.10
  128.6 6.5 %copy-start.2 = (bf16[1536,256]{0,1:T(8,128)(2,1)}, bf16[1536,256]{0,1:T(8,128)(2,1)S(1)}, u32[]{:S(2)}) copy-start(bf16[1536,256]{0,1:T(8,128)(2,1)S(1)} %get-tuple-element.111) | copy-start | bytes 2359300
  135.1 2.3 copy-start.5
  148.8 95.5 %copy-start.3 = (bf16[1536,256]{0,1:T(8,128)(2,1)S(1)}, bf16[1536,256]{0,1:T(8,128)(2,1)}, u32[]{:S(2)}) copy-start(bf16[1536,256]{0,1:T(8,128)(2,1)} %copy-done.2) | copy-start | bytes 2359300
  237.2 27.1 %all-to-all-start = ((f32[16,1,352]{2,1,0:T(1,128)}), f32[16,1,352]{2,1,0:T(1,128)S(1)}, u32[]{:S(2)}, u32[]{:S(2)}) async-start(f32[16,1,352]{2,1,0:T(1,128)} %all_to_all.8), calls=%async_computation | async-start | bytes 49152 | tf_op jit(solution)/shard_map/all_to_all | solution.py:553
  244.3 4.8 %copy-start.6 = (bf16[1536,256]{0,1:T(8,128)(2,1)S(1)}, bf16[1536,256]{0,1:T(8,128)(2,1)}, u32[]{:S(2)}) copy-start(bf16[1536,256]{0,1:T(8,128)(2,1)} %get-tuple-element.112) | copy-start | bytes 2359300
  244.3 10.8 %slice-start.2 = ((s8[6291456]{0:T(1024)(128)(4,1)}), s8[4194304]{0:T(1024)(128)(4,1)S(1)}, s32[]{:S(2)}) async-start(s8[6291456]{0:T(1024)(128)(4,1)} %bitcast.74), calls=%async_computation.3 | async-start | bytes 8388608
  249.1 6.1 %slice-start.3 = ((s8[6291456]{0:T(1024)(128)(4,1)}), s8[2097152]{0:T(1024)(128)(4,1)S(1)}, s32[]{:S(2)}) async-start(s8[6291456]{0:T(1024)(128)(4,1)} %bitcast.74), calls=%async_computation.4 | async-start | bytes 4194304
  249.1 6.1 %copy-start.11 = (bf16[1536,256]{0,1:T(8,128)(2,1)S(1)}, bf16[1536,256]{0,1:T(8,128)(2,1)}, u32[]{:S(2)}) copy-start(bf16[1536,256]{0,1:T(8,128)(2,1)} %get-tuple-element.108) | copy-start | bytes 2359300
  261.8 9.9 %copy-start.1 = (bf16[1,2048,256]{2,1,0:T(8,128)(2,1)S(1)}, bf16[1,2048,256]{2,1,0:T(8,128)(2,1)}, u32[]{:S(2)}) copy-start(bf16[1,2048,256]{2,1,0:T(8,128)(2,1)} %param.14) | copy-start | bytes 3145732
  261.8 7.4 %copy-start.7 = (s32[256,4]{0,1:T(4,128)S(1)}, s32[256,4]{0,1:T(4,128)}, u32[]{:S(2)}) copy-start(s32[256,4]{0,1:T(4,128)} %param.11) | copy-start | bytes 12292
  261.8 7.5 %copy-start.8 = (f32[256,4]{0,1:T(4,128)S(1)}, f32[256,4]{0,1:T(4,128)}, u32[]{:S(2)}) copy-start(f32[256,4]{0,1:T(4,128)} %param.12) | copy-start | bytes 12292

commit v4 on v3

--- a/solution.py
+++ b/solution.py
@@ -60,13 +60,16 @@
 
 def combine_kernel(
     planes, width,
-    own, oth, sh_own, sh_oth, scatter, grads,
+    parts, sh_parts, scatter, grads,
     tok_out, grad_out,
     tp_in, sh_in, sums, plane_in, gplane_in, z_out, z_in, gz_out, gz_in, routed, gtotal,
     tp_sem, plane_sem, gplane_sem, z_sem, gz_sem,
 ):
     me, core = lax.axis_index("ep"), lax.axis_index("tp")
     z, q = me // width, me % width
+    cols = tok_out.shape[1]
+    mine = pl.ds(pl.multiple_of(core * cols, cols), cols)
+    other = pl.ds(pl.multiple_of((1 - core) * cols, cols), cols)
     order = list(range(1, planes)) + [0]
     dest_z = [(z + step) % planes for step in order]
     dest_q = [(q + step) % width for step in range(width)]
@@ -78,11 +81,11 @@
         return copy
 
     tp_copies = [
-        start(copy_to(oth.at[dest_z[i]], tp_in.at[i], tp_sem.at[0, i], tp_sem.at[1, i], me, 1 - core))
+        start(copy_to(parts.at[dest_z[i], :, :, other], tp_in.at[i], tp_sem.at[0, i], tp_sem.at[1, i], me, 1 - core))
         for i in range(planes)
     ]
     sh_copy = start(
-        copy_to(sh_oth, sh_in, tp_sem.at[0, planes], tp_sem.at[1, planes], me, 1 - core)
+        copy_to(sh_parts.at[:, other], sh_in, tp_sem.at[0, planes], tp_sem.at[1, planes], me, 1 - core)
     )
     plane_copies, gplane_copies = {}, {}
     for i in range(planes):
@@ -101,7 +104,7 @@
         tp_copies[i].wait_recv()
         for d in range(width):
             sums[i, d] = (
-                own[dest_z[i], dest_q[d]].astype(F32) + tp_in[i, dest_q[d]].astype(F32)
+                parts[dest_z[i], dest_q[d], :, mine].astype(F32) + tp_in[i, dest_q[d]].astype(F32)
             ).astype(BF16)
             if d:
                 peer = z * width + dest_q[d]
@@ -152,16 +155,15 @@
         total = total + gz_in[i].astype(F32)
         acc = acc + z_in[i].astype(F32)
     grad_out[...] = total
-    acc = acc + (sh_own[...].astype(F32) + sh_in[...].astype(F32))
+    acc = acc + (sh_parts[:, mine].astype(F32) + sh_in[...].astype(F32))
     tok_out[...] = acc.astype(BF16)
     for copy in started:
         copy.wait_send()
 
 
-def combine(planes, own, oth, sh_own, sh_oth, scatter, grads):
-    width = own.shape[1]
-    cap, cols = own.shape[2:]
-    rows = sh_own.shape[0]
+def combine(planes, cols, parts, sh_parts, scatter, grads):
+    width, cap = parts.shape[1:3]
+    rows = sh_parts.shape[0]
     g_shape = grads.shape[2:]
     vmem = pl.BlockSpec(memory_space=pltpu.VMEM)
     far, side = max(planes - 1, 1), max(width - 1, 1)
@@ -171,7 +173,7 @@
             jax.ShapeDtypeStruct((rows, cols), BF16),
             jax.ShapeDtypeStruct(g_shape, F32),
         ),
-        in_specs=[vmem] * 6,
+        in_specs=[vmem] * 4,
         out_specs=(vmem, vmem),
         scratch_shapes=[
             pltpu.VMEM((planes, width, cap, cols), BF16),
@@ -192,10 +194,10 @@
             pltpu.SemaphoreType.DMA((2, far)),
         ],
         compiler_params=pltpu.CompilerParams(
-            has_side_effects=True, vmem_limit_bytes=60 * 2**20
+            has_side_effects=True, vmem_limit_bytes=40 * 2**20
         ),
         name="combine",
-    )(own, oth, sh_own, sh_oth, scatter, grads)
+    )(parts, sh_parts, scatter, grads)
 
 
 def dispatch_kernel(
@@ -468,7 +470,7 @@
             pltpu.SemaphoreType.DMA((2, planes, width, 2)),
         ],
         compiler_params=pltpu.CompilerParams(
-            has_side_effects=True, vmem_limit_bytes=60 * 2**20
+            has_side_effects=True, vmem_limit_bytes=40 * 2**20
         ),
         name="dispatch",
     )(x, table, *shared)
@@ -521,17 +523,9 @@
     line_rank = line_table[:, 0][:, senders]
     scatter = (line_rank[..., None] == slots.astype(F32)).astype(BF16)
 
-    def halves(values):
-        return (
-            lax.dynamic_slice_in_dim(values, first_col, half_cols, 1),
-            lax.dynamic_slice_in_dim(values, half_cols - first_col, half_cols, 1),
-        )
-
-    own, oth = halves(routed_part)
-    sh_own, sh_oth = halves(shared_part)
-    blocks = (planes, width, capacity, half_cols)
+    blocks = (planes, width, capacity, model_width)
     token_grad, shared_sum = combine(
-        planes, own.reshape(blocks), oth.reshape(blocks), sh_own, sh_oth, scatter, grads
+        planes, half_cols, routed_part.reshape(blocks), shared_part, scatter, grads
     )
     out_g = shared_sum[:part_rows]
     out_u = shared_sum[part_rows : 2 * part_rows]

time: 272 us -> 257 us (0.945)
  Pallas kernels: 196 us -> 186 us
  other arithmetic: 8.35 us -> 4.79 us
    dynamic_slice x2 -> x0, local copies, waits for them, and re-layouts: 5.7 us -> none  [halves(): lax.dynamic_slice_in_dim(values, half_cols - first_col, half_cols, 1)]
    pallas_call x1, Pallas kernels: 85.6 us -> 80.3 us  [combine(): pl.pallas_call(functools.partial(combine_kernel, planes, width), out_shap...]
    pallas_call x1, Pallas kernels: 111 us -> 106 us  [dispatch(): pl.pallas_call(functools.partial(dispatch_kernel, planes, width, cap), ou...]
    unnamed x36 -> x46, local copies, waits for them, and re-layouts: 7.08 us -> 11 us
  transfers between devices with their start and end apart: 1 -> 1, of which waited for: 0 -> 0; matrix products, arithmetic and copies ran while one was open for 7% -> 9% of each run, Pallas kernels for 0% -> 0%
where the time goes in v4:
time: 257 us
  Pallas kernels  186 us (72%)
  matrix products  39.3 us (15%)
  local copies, waits for them, and re-layouts  14.7 us (6%)
  starting transfers between devices  7.13 us (3%)
  other arithmetic  4.79 us (2%)
  blocking collectives  3.97 us (2%)
    pallas_call x1, Pallas kernels, dispatch(): pl.pallas_call(functools.partial(dispatch_kernel, planes, width, cap), ou...  106 us
    pallas_call x1, Pallas kernels, combine(): pl.pallas_call(functools.partial(combine_kernel, planes, width), out_shap...  80.3 us
    unnamed x46, local copies, waits for them, and re-layouts  11 us
    all_to_all x1, starting transfers between devices, local(): small = lax.all_to_all(small, 'ep', split_axis=0, concat_axis=0, tiled=True)  7.13 us
    dot_general x1, matrix products, expert_backward(): jnp.dot(d_up, w_u.T, preferred_element_type=F32)  6.6 us
    dot_general x1, matrix products, expert_backward(): jnp.dot(d_gate, w_g.T, preferred_element_type=F32)  6.43 us
    dot_general x1, matrix products, expert_backward(): lax.dot_general(inputs, d_gate, contract, preferred_element_type=F32)  6.08 us
    dot_general x1, matrix products, expert_backward(): grad_u = lax.dot_general(inputs, d_up, contract, preferred_element_type=F32)  6.05 us
  transfers between devices with their start and end apart: 1, of which 0 were waited for; matrix products, arithmetic and copies ran while one was open for 9% of the time, Pallas kernels for 0%

profile of v4, /device:TPU:0, one launch (start us, length us, event | category | flops | bytes accessed | tf_op | source)
XLA Modules:
  0.0 257.1 jit_solution(8347262958498721919)
XLA Ops:
  0.8 0.8 fusion.16
  1.5 0.2 fusion.1
  1.8 0.8 select_reduce_fusion.2
  2.6 1.4 constant_dynamic-slice_fusion
  4.1 0.3 copy-done.4
  4.4 0.3 copy-done.5
  4.7 0.3 copy-done.6
  5.0 1.2 copy-done.7
  6.3 105.9 %dispatch.1 = (bf16[4,4,96,2048]{3,2,1,0:T(8,128)(2,1)}, bf16[4,4,96,2048]{3,2,1,0:T(8,128)(2,1)}, f32[4,2,16,256]{3,2,1,0:T(8,128)S(1)}, bf16[4,4,384,256]{3,2,1,0:T(8,128)(2,1)S(1)}, bf16[256,2048]{1,0:T(8,128)(2,1)S(1)}) custom-call(bf16[256,2048]{1,0:T(8,128)(2,1)S(1)} %pad_maximum_fusion.x, f32[2,16,256]{2,1,0:T(8,128)S(1)} %pad_maximum_fusion.1.table, ...), custom_call_target="tpu_custom_call" | custom-call | tf_op jit(solution)/shard_map/dispatch/pallas_call | solution.py:452
  112.2 1.7 copy-done.1
  114.0 0.6 gather_fusion
  114.6 4.8 %fusion.4 = f32[1536,256]{0,1:T(8,128)S(1)} fusion(bf16[1536,2048]{1,0:T(8,128)(2,1)} %bitcast.75, bf16[1,2048,256]{2,1,0:T(8,128)(2,1)S(1)} %copy-done), kind=kOutput, calls=%fused_computation.19 | convolution fusion | flops 1610612736 | bytes 8912896 | tf_op jit(solution)/shard_map/dot_general | solution.py:21
  119.5 1.9 fusion.7
  121.8 3.6 %multiply_reduce_fusion.3 = (f32[1536]{0:T(1024)S(1)}, bf16[1536,256]{0,1:T(8,128)(2,1)}, bf16[1536,256]{0,1:T(8,128)(2,1)S(1)}, bf16[1536,256]{0,1:T(8,128)(2,1)}) fusion(f32[1536,256]{0,1:T(8,128)S(1)} %fusion.7, f32[1536,256]{0,1:T(8,128)S(1)} %fusion.4, bf16[1536,2048]{1,0:T(8,128)(2,1)S(1)} %bitcast.71, bf16[1,256,2048]{2,1,0:T(8,128)(2,1)S(1)} %copy-done.15), kind=kOutput, calls=%fused_computation.7 | convolution fusion | flops 1617689088 | bytes 12851200 | tf_op jit(solution)/shard_map/dot_general | solution.py:25
  125.5 6.4 %fusion.2 = f32[1536,2048]{1,0:T(8,128)} fusion(bf16[1536,256]{0,1:T(8,128)(2,1)S(1)} %get-tuple-element.109, bf16[1,2048,256]{2,1,0:T(8,128)(2,1)S(1)} %copy-done), kind=kOutput, calls=%fused_computation.17 | convolution fusion | flops 1610612736 | bytes 14417920 | tf_op jit(solution)/shard_map/dot_general | solution.py:33
  131.9 0.6 compare_convert_fusion.scatter
  132.5 6.6 %add_convert_fusion = bf16[1536,2048]{1,0:T(8,128)(2,1)S(1)} fusion(f32[1536,2048]{1,0:T(8,128)} %fusion.2, bf16[1536,256]{0,1:T(8,128)(2,1)S(1)} %copy-done.10, bf16[1,2048,256]{2,1,0:T(8,128)(2,1)S(1)} %copy-done.9), kind=kOutput, calls=%fused_computation.1 | convolution fusion | flops 1616904192 | bytes 20709376 | tf_op jit(solution)/shard_map/dot_general | solution.py:33
  139.2 80.3 %combine.1 = (bf16[256,1024]{1,0:T(8,128)(2,1)S(1)}, f32[384,256]{1,0:T(8,128)S(1)}) custom-call(bf16[4,4,96,2048]{3,2,1,0:T(8,128)(2,1)S(1)} %bitcast.56, bf16[256,2048]{1,0:T(8,128)(2,1)S(1)} %get-tuple-element.23.sh_parts, bf16[4,4,256,96]{3,2,1,0:T(8,128)(2,1)S(1)} %compare_convert_fusion.scatter, bf16[4,4,384,256]{3,2,1,0:T(8,128)(2,1)S(1)} %copy-done.2), custom_call_target="tpu_custom_call" | custom-call | tf_op jit(solution)/shard_map/combine/pallas_call | solution.py:170
  219.5 0.7 multiply_reduce_fusion.4
  220.6 0.7 all_to_all.8
  221.3 7.1 %all-to-all-start = ((f32[16,1,352]{2,1,0:T(1,128)}), f32[16,1,352]{2,1,0:T(1,128)S(1)}, u32[]{:S(2)}, u32[]{:S(2)}) async-start(f32[16,1,352]{2,1,0:T(1,128)} %all_to_all.8), calls=%async_computation | async-start | bytes 49152 | tf_op jit(solution)/shard_map/all_to_all | solution.py:547
  228.5 6.1 %multiply_reduce_fusion.2 = (f32[2048]{0:T(1024)S(1)}, f32[2048,256]{0,1:T(8,128)}) fusion(bf16[1536,256]{0,1:T(8,128)(2,1)S(1)} %get-tuple-element.109, bf16[1536,2048]{1,0:T(8,128)(2,1)} %bitcast.76), kind=kOutput, calls=%fused_computation.4 | convolution fusion | flops 1611659264 | bytes 9183232 | tf_op jit(solution)/shard_map/dot_general | solution.py:30
  234.5 6.0 %multiply_reduce_fusion.1 = (f32[2048]{0:T(1024)S(1)}, f32[2048,256]{0,1:T(8,128)}) fusion(bf16[1536,256]{0,1:T(8,128)(2,1)S(1)} %copy-done.11, bf16[1536,2048]{1,0:T(8,128)(2,1)} %bitcast.77), kind=kOutput, calls=%fused_computation.3 | convolution fusion | flops 1611659264 | bytes 9183232 | tf_op jit(solution)/shard_map/dot_general | solution.py:31
  240.6 3.7 %multiply_reduce_fusion = (f32[256]{0:T(256)}, f32[256,2048]{1,0:T(8,128)}) fusion(bf16[1536,256]{0,1:T(8,128)(2,1)S(1)} %copy-done.16, bf16[1536,2048]{1,0:T(8,128)(2,1)S(1)} %bitcast.74), kind=kOutput, calls=%fused_computation.2 | convolution fusion | flops 1611661056 | bytes 9176064 | tf_op jit(solution)/shard_map/dot_general | solution.py:32
  244.3 2.9 %copy.56 = f32[1,2048,256]{2,1,0:T(8,128)} copy(f32[1,2048,256]{1,2,0:T(8,128)} %bitcast.58) | data formatting | bytes 4194304
  247.2 2.9 %copy.55 = f32[1,2048,256]{2,1,0:T(8,128)} copy(f32[1,2048,256]{1,2,0:T(8,128)} %bitcast.57) | data formatting | bytes 4194304
  250.1 0.7 copy.54
  250.8 0.7 slice_reduce_fusion
  251.4 4.0 %all-reduce = (f32[16,96]{1,0:T(8,128)S(1)}, f32[1,2048]{1,0:T(1,128)}, f32[1,2048]{1,0:T(1,128)}, f32[128]{0:T(128)}, f32[128]{0:T(128)}) all-reduce(f32[16,96]{1,0:T(8,128)S(1)} %slice.26, f32[1,2048]{1,0:T(1,128)S(1)} %bitcast.66, f32[1,2048]{1,0:T(1,128)S(1)} %bitcast.67, ...), channel_id=1, replica_groups=mesh['ep'=16,'tp'=2] {'tp'}, use_global_device_ids=true, to_apply=%region_4.5 | all-reduce | flops 5888 | bytes 47104 | tf_op jit(solution)/shard_map/psum | solution.py:548
  255.4 0.3 select_reduce_fusion
  255.7 0.6 div.18
  256.3 0.8 copy.61
  (59 shorter events, 1.2 us)
Async XLA Ops:
  0.6 113.9 %copy-start = (bf16[1,2048,256]{2,1,0:T(8,128)(2,1)S(1)}, bf16[1,2048,256]{2,1,0:T(8,128)(2,1)}, u32[]{:S(2)}) copy-start(bf16[1,2048,256]{2,1,0:T(8,128)(2,1)} %param.14) | copy-start | bytes 3145732
  2.5 1.6 copy-start.3
  2.6 1.8 copy-start.4
  2.6 2.2 copy-start.5
  2.6 2.5 copy-start.6
  5.0 1.2 copy-start.7
  112.2 1.8 copy-start.1
  114.6 4.8 %copy-start.8 = (bf16[1,2048,256]{2,1,0:T(8,128)(2,1)S(1)}, bf16[1,2048,256]{2,1,0:T(8,128)(2,1)}, u32[]{:S(2)}) copy-start(bf16[1,2048,256]{2,1,0:T(8,128)(2,1)} %param.15) | copy-start | bytes 3145732
  114.6 4.9 %copy-start.14 = (bf16[4,4,96,2048]{3,2,1,0:T(8,128)(2,1)S(1)}, bf16[4,4,96,2048]{3,2,1,0:T(8,128)(2,1)}, u32[]{:S(2)}) copy-start(bf16[4,4,96,2048]{3,2,1,0:T(8,128)(2,1)} %get-tuple-element.22) | copy-start | bytes 18874372
  114.6 6.8 %slice-start = ((s8[6291456]{0:T(1024)(128)(4,1)}), s8[4194304]{0:T(1024)(128)(4,1)S(1)}, s32[]{:S(2)}) async-start(s8[6291456]{0:T(1024)(128)(4,1)} %bitcast.69), calls=%async_computation.1 | async-start | bytes 8388608
  119.5 2.0 slice-start.1
  119.5 2.2 copy-start.15
  125.5 7.0 %copy-start.9 = (bf16[1,2048,256]{2,1,0:T(8,128)(2,1)S(1)}, bf16[1,2048,256]{2,1,0:T(8,128)(2,1)}, u32[]{:S(2)}) copy-start(bf16[1,2048,256]{2,1,0:T(8,128)(2,1)} %param.15) | copy-start | bytes 3145732
  125.5 7.1 %copy-start.10 = (bf16[1536,256]{0,1:T(8,128)(2,1)S(1)}, bf16[1536,256]{0,1:T(8,128)(2,1)}, u32[]{:S(2)}) copy-start(bf16[1536,256]{0,1:T(8,128)(2,1)} %get-tuple-element.110) | copy-start | bytes 2359300
  132.5 6.6 %copy-start.2 = (bf16[4,4,384,256]{3,2,1,0:T(8,128)(2,1)S(1)}, bf16[4,4,384,256]{3,2,1,0:T(8,128)(2,1)}, u32[]{:S(2)}) copy-start(bf16[4,4,384,256]{3,2,1,0:T(8,128)(2,1)} %copy-done.1) | copy-start | bytes 9437188
  221.3 29.5 %all-to-all-start = ((f32[16,1,352]{2,1,0:T(1,128)}), f32[16,1,352]{2,1,0:T(1,128)S(1)}, u32[]{:S(2)}, u32[]{:S(2)}) async-start(f32[16,1,352]{2,1,0:T(1,128)} %all_to_all.8), calls=%async_computation | async-start | bytes 49152 | tf_op jit(solution)/shard_map/all_to_all | solution.py:547
  228.4 6.1 %copy-start.11 = (bf16[1536,256]{0,1:T(8,128)(2,1)S(1)}, bf16[1536,256]{0,1:T(8,128)(2,1)}, u32[]{:S(2)}) copy-start(bf16[1536,256]{0,1:T(8,128)(2,1)} %get-tuple-element.110) | copy-start | bytes 2359300
  228.4 12.1 %slice-start.2 = ((s8[6291456]{0:T(1024)(128)(4,1)}), s8[4194304]{0:T(1024)(128)(4,1)S(1)}, s32[]{:S(2)}) async-start(s8[6291456]{0:T(1024)(128)(4,1)} %bitcast.72), calls=%async_computation.3 | async-start | bytes 8388608
  234.5 6.1 %slice-start.3 = ((s8[6291456]{0:T(1024)(128)(4,1)}), s8[2097152]{0:T(1024)(128)(4,1)S(1)}, s32[]{:S(2)}) async-start(s8[6291456]{0:T(1024)(128)(4,1)} %bitcast.72), calls=%async_computation.4 | async-start | bytes 4194304
  234.5 6.1 %copy-start.16 = (bf16[1536,256]{0,1:T(8,128)(2,1)S(1)}, bf16[1536,256]{0,1:T(8,128)(2,1)}, u32[]{:S(2)}) copy-start(bf16[1536,256]{0,1:T(8,128)(2,1)} %get-tuple-element.108) | copy-start | bytes 2359300
  247.2 8.5 %copy-start.12 = (s32[256,4]{0,1:T(4,128)S(1)}, s32[256,4]{0,1:T(4,128)}, u32[]{:S(2)}) copy-start(s32[256,4]{0,1:T(4,128)} %param.11) | copy-start | bytes 12292
  247.2 8.6 %copy-start.13 = (f32[256,4]{0,1:T(4,128)S(1)}, f32[256,4]{0,1:T(4,128)}, u32[]{:S(2)}) copy-start(f32[256,4]{0,1:T(4,128)} %param.12) | copy-start | bytes 12292
